TPU v7x, 32 devices: a whole 2x2x4 slice. The times are simulated.
32 devices in a mesh: sp: 16 (over z, y, x), tp: 2 (over core).
Axes of the slice: x: 2, y: 2, z: 4, core: 2. Of those that a mesh axis runs over, the one named last changes fastest.
Arguments:
- tokens: bfloat16 [6144, 2048], P('sp', 'tp'), may hold values from -6 to 6
- input_gain: float32 [2048], replicated, may hold values from 0.1 to 1.9
- query_weight: bfloat16 [2048, 1024], P(None, 'tp'), may hold values from -0.5 to 0.5
- query_rot_weight: bfloat16 [2048, 512], P(None, 'tp'), may hold values from -0.125 to 0.125
- kv_down: bfloat16 [2048, 256], replicated, may hold values from -0.5 to 0.5
- rot_down: bfloat16 [2048, 32], replicated, may hold values from -0.125 to 0.125
- kv_gain: float32 [256], replicated, may hold values from 0.1 to 1.9
- key_up: bfloat16 [256, 1024], P(None, 'tp'), may hold values from -0.5 to 0.5
- value_up: bfloat16 [256, 1024], P(None, 'tp'), may hold values from -4 to 4
- conv_value_weight: bfloat16 [2048, 1024], P(None, 'tp'), may hold values from -0.125 to 0.125
- conv_gate_weight: bfloat16 [2048, 1024], P(None, 'tp'), may hold values from -0.125 to 0.125
- conv_taps: float32 [31, 1024], P(None, 'tp'), may hold values from -8 to 8
- conv_ln_gain: float32 [1024], P('tp'), may hold values from 0.1 to 1.9
- conv_ln_bias: float32 [1024], P('tp'), may hold values from -3 to 3
- att_out_gain: float32 [1024], P('tp'), may hold values from 0.1 to 1.9
- conv_out_gain: float32 [1024], P('tp'), may hold values from 0.1 to 1.9
- att_out_weight: bfloat16 [1024, 2048], P('tp'), may hold values from -0.125 to 0.125
- conv_out_weight: bfloat16 [1024, 2048], P('tp'), may hold values from -0.125 to 0.125
Outputs:
- mixed: bfloat16 [6144, 2048], P('sp', 'tp')
All inputs are finite; a program needn't handle non-finite values.
Results may differ from a plain program's by a relative error of at most 0.017.
Values may be sent and summed in bfloat16 or wider, within the bound.
A program may use at most 128 MiB of HBM per device.

v0:
```python
import math

import jax
import jax.numpy as jnp
from jax import lax
from jax.experimental import pallas as pl
from jax.experimental.pallas import tpu as pltpu
from jax.sharding import PartitionSpec as P

D_MODEL = 2048
NOPE_DIM = 64
ROT_DIM = 32
VALUE_DIM = 64
CONV_CH = 1024
KERNEL = 31
ATT_WIDTH = 1024


norm_eps = 1e-06
far_below = -1e30
rope_base = 10000.0


def shifted(block, axis, distance):
    devices = range(lax.axis_size(axis))
    route = [(i - distance, i) for i in devices if i - distance in devices]
    return lax.ppermute(block, axis, route)


def rotary_tables(positions, half_dim):
    frequency = rope_base ** (-jnp.arange(half_dim, dtype=jnp.float32) / half_dim)
    angles = positions.astype(jnp.float32)[:, None] * frequency[None, :]
    return (jnp.cos(angles), jnp.sin(angles))


def rotate_half(values, cos_table, sine_table):
    half_dim = cos_table.shape[-1]
    front_half = values[..., :half_dim]
    back_half = values[..., half_dim:]
    return jnp.concatenate(
        [
            front_half * cos_table - back_half * sine_table,
            back_half * cos_table + front_half * sine_table,
        ],
        axis=-1,
    )


MESH = pl.DeviceIdType.MESH


def push(src, dst, send, recv, target):
    return pltpu.make_async_remote_copy(
        src_ref=src,
        dst_ref=dst,
        send_sem=send,
        recv_sem=recv,
        device_id=target,
        device_id_type=MESH,
    )


def greet(targets):
    barrier = pltpu.get_barrier_semaphore()
    for target in targets:
        pl.semaphore_signal(barrier, inc=1, device_id=target, device_id_type=MESH)
    pl.semaphore_wait(barrier, len(targets))


def other_core():
    return {"sp": lax.axis_index("sp"), "tp": 1 - lax.axis_index("tp")}


def front_kernel(
    tok_ref, gain_ref, kv_gain_ref, cos_ref, sin_ref, taps_ref, ln_gain_ref, ln_bias_ref,
    qw_hbm, qrw_hbm, kvd_hbm, rotw_hbm, cvw_hbm, cgw_hbm,
    q_ref, packed_ref, swish_ref,
    qw, qrw, kvd, rotw, cvw, cgw, scaled, landed, narrow, gated, rim, wide, conv,
    sq_mine, sq_other, w_sem, tok_send, tok_recv, rim_send, rim_recv, sq_send, sq_recv,
):
    mine = lax.axis_index("tp")
    seat = lax.axis_index("sp")
    seats = lax.axis_size("sp")
    rows, width = tok_ref.shape
    heads, _, lanes = q_ref.shape
    loads = [
        pltpu.make_async_copy(src, dst, w_sem.at[index])
        for index, (src, dst) in enumerate(
            (
                (kvd_hbm, kvd), (rotw_hbm, rotw), (cvw_hbm, cvw),
                (cgw_hbm, cgw), (qw_hbm, qw), (qrw_hbm, qrw),
            )
        )
    ]
    for load in loads:
        load.start()
    ahead = {"sp": (seat + 1) % seats, "tp": mine}
    behind = {"sp": (seat + seats - 1) % seats, "tp": mine}
    greet([other_core(), ahead, behind])
    copy = push(tok_ref, landed, tok_send, tok_recv, other_core())
    copy.start()

    def place(block, index):
        cols = pl.ds(pl.multiple_of(index * width, 128), width)
        full = block[...].astype(jnp.float32)
        scaled[:, cols] = (full * gain_ref[:, cols]).astype(jnp.bfloat16)
        return jnp.sum(full * full, axis=1, keepdims=True)

    squares = place(tok_ref, mine)
    copy.wait()
    squares = squares + place(landed, 1 - mine)
    row_scale = lax.rsqrt(squares / (2 * width) + norm_eps)

    def project(weight):
        return jnp.dot(scaled[...], weight[...], preferred_element_type=jnp.float32)

    loads[2].wait()
    loads[3].wait()
    gate = project(cgw) * row_scale
    gated[...] = (project(cvw) * row_scale * jax.nn.sigmoid(gate)).astype(jnp.bfloat16)
    edge = rim.shape[0]
    rim_copy = push(gated.at[pl.ds(rows - edge, edge)], rim, rim_send, rim_recv, ahead)

    @pl.when(seat < seats - 1)
    def _():
        rim_copy.start()

    loads[0].wait()
    loads[1].wait()
    raw = project(kvd)
    rank = raw.shape[1]
    latent = (
        raw
        * lax.rsqrt(jnp.mean(raw * raw, axis=1, keepdims=True) + norm_eps)
        * kv_gain_ref[...]
    )
    packed_ref[:rank, :] = latent.T.astype(jnp.bfloat16)
    cos_table = cos_ref[...]
    sin_table = sin_ref[...]
    turn = cos_table.shape[0]

    def rotate(block):
        front = block[:turn]
        back = block[turn : 2 * turn]
        return jnp.concatenate(
            [front * cos_table - back * sin_table, back * cos_table + front * sin_table], axis=0
        )

    narrow[...] = jnp.broadcast_to(row_scale, narrow.shape)
    key_turn = lax.dot_general(
        rotw[...], scaled[...], (((1,), (1,)), ((), ())), preferred_element_type=jnp.float32
    )
    packed_ref[rank:, :] = rotate(key_turn * narrow[...].T[: 2 * turn]).astype(jnp.bfloat16)
    loads[4].wait()
    loads[5].wait()
    query_scale = row_scale * (math.log2(math.e) / math.sqrt(NOPE_DIM + ROT_DIM))
    plain = (project(qw) * query_scale).T
    turned = (project(qrw) * query_scale).T
    blank = jnp.zeros((lanes - NOPE_DIM - ROT_DIM, rows), jnp.float32)
    for head in range(heads):
        column = jnp.concatenate(
            [
                plain[head * NOPE_DIM : (head + 1) * NOPE_DIM],
                rotate(turned[head * ROT_DIM : (head + 1) * ROT_DIM]),
                blank,
            ],
            axis=0,
        )
        q_ref[head] = column.T.astype(jnp.bfloat16)

    @pl.when(seat > 0)
    def _():
        rim_copy.wait_recv()

    @pl.when(seat == 0)
    def _():
        rim[...] = jnp.zeros(rim.shape, jnp.bfloat16)

    taps = taps_ref.shape[0]
    chunk = 64
    for part in range(conv.shape[1] // 128):
        cols = slice(part * 128, (part + 1) * 128)
        wide[part, :edge, :] = rim[:, cols].astype(jnp.float32)
        wide[part, edge:, :] = gated[:, cols].astype(jnp.float32)
        coeff = taps_ref[:, cols]

        def band(step, carry, part=part, cols=cols, coeff=coeff):
            base = step * chunk
            total = jnp.zeros((chunk, 128), jnp.float32)
            for tap in range(taps):
                total = total + coeff[tap : tap + 1, :] * wide[
                    part, pl.ds(base + (edge - taps + 1 + tap), chunk), :
                ]
            conv[pl.ds(pl.multiple_of(base, chunk), chunk), cols] = total
            return carry

        lax.fori_loop(0, rows // chunk, band, 0)

    values = conv[...]
    for slot, total in enumerate((values, values * values)):
        sq_mine[:, slot * 128 : (slot + 1) * 128] = jnp.broadcast_to(
            jnp.sum(total, axis=1, keepdims=True), (rows, 128)
        )
    sums = push(sq_mine, sq_other, sq_send, sq_recv, other_core())
    sums.start()
    sums.wait()
    moments = (sq_mine[...] + sq_other[...]) / CONV_CH
    mean_val = moments[:, :1]
    spread = moments[:, 128:129] - mean_val * mean_val
    normed = (values - mean_val) * lax.rsqrt(spread + norm_eps)
    swish_ref[...] = jax.nn.silu(normed * ln_gain_ref[...] + ln_bias_ref[...])

    @pl.when(seat < seats - 1)
    def _():
        rim_copy.wait_send()


def front(tokens, gain, kv_gain, cos_t, sin_t, taps, ln_gain, ln_bias, weights):
    rows, width = tokens.shape
    chans = taps.shape[1]
    heads = weights[0].shape[1] // NOPE_DIM
    rank = weights[2].shape[1]
    vmem = pl.BlockSpec(memory_space=pltpu.VMEM)
    anywhere = pl.BlockSpec(memory_space=pltpu.HBM)
    dma = pltpu.SemaphoreType.DMA
    edge = 32
    return pl.pallas_call(
        front_kernel,
        out_shape=(
            jax.ShapeDtypeStruct((heads, rows, 128), jnp.bfloat16),
            jax.ShapeDtypeStruct((rank + ROT_DIM, rows), jnp.bfloat16),
            jax.ShapeDtypeStruct((rows, chans), jnp.float32),
        ),
        in_specs=[vmem] * 8 + [anywhere] * 6,
        out_specs=(vmem,) * 3,
        scratch_shapes=[pltpu.VMEM(weight.shape, jnp.bfloat16) for weight in weights]
        + [
            pltpu.VMEM((rows, 2 * width), jnp.bfloat16),
            pltpu.VMEM((rows, width), jnp.bfloat16),
            pltpu.VMEM((rows, 128), jnp.float32),
            pltpu.VMEM((rows, chans), jnp.bfloat16),
            pltpu.VMEM((edge, chans), jnp.bfloat16),
            pltpu.VMEM((chans // 128, rows + edge, 128), jnp.float32),
            pltpu.VMEM((rows, chans), jnp.float32),
            pltpu.VMEM((rows, 256), jnp.float32),
            pltpu.VMEM((rows, 256), jnp.float32),
            dma((6,)),
        ]
        + [dma] * 6,
        compiler_params=pltpu.CompilerParams(
            vmem_limit_bytes=62 << 20, collective_id=0, has_side_effects=True
        ),
        name="front",
    )(tokens, gain, kv_gain, cos_t, sin_t, taps, ln_gain, ln_bias, *weights)


def output_kernel(
    att_ref, swish_ref, att_gain, conv_gain, att_hbm, conv_hbm, out_ref,
    att_w, conv_w, sq_mine, sq_other, part, landed, w_sem, sq_send, sq_recv, send, recv,
):
    loads = [
        pltpu.make_async_copy(att_hbm, att_w, w_sem.at[0]),
        pltpu.make_async_copy(conv_hbm, conv_w, w_sem.at[1]),
    ]
    for load in loads:
        load.start()
    mine = lax.axis_index("tp")
    rows, width = out_ref.shape
    lanes = sq_mine.shape[1] // 2
    attended = att_ref[...].astype(jnp.float32)
    swished = swish_ref[...]
    for slot, value in enumerate((attended, swished)):
        total = jnp.sum(value * value, axis=1, keepdims=True)
        sq_mine[:, slot * lanes : (slot + 1) * lanes] = jnp.broadcast_to(total, (rows, lanes))
    greet([other_core()])
    sums = push(sq_mine, sq_other, sq_send, sq_recv, other_core())
    sums.start()
    sums.wait()
    sq = sq_mine[...] + sq_other[...]
    att_scale = lax.rsqrt(sq[:, :1] / ATT_WIDTH + norm_eps)
    conv_scale = lax.rsqrt(sq[:, lanes : lanes + 1] / CONV_CH + norm_eps)
    att_mixed = (attended * att_scale * att_gain[...]).astype(jnp.bfloat16)
    conv_mixed = (swished * conv_scale * conv_gain[...]).astype(jnp.bfloat16)
    piece = part.shape[2]
    pieces = part.shape[0]

    def product(owner, index):
        cols = pl.ds(pl.multiple_of(owner * width + index * piece, 128), piece)
        return (
            jnp.dot(att_mixed, att_w[:, cols], preferred_element_type=jnp.float32)
            + jnp.dot(conv_mixed, conv_w[:, cols], preferred_element_type=jnp.float32)
        ).astype(jnp.bfloat16)

    for load in loads:
        load.wait()
    copies = []
    for index in range(pieces):
        part[index] = product(1 - mine, index)
        copy = push(
            part.at[index], landed.at[index], send.at[index], recv.at[index], other_core()
        )
        copy.start()
        copies.append(copy)
    for index in range(pieces):
        own = product(mine, index).astype(jnp.float32)
        copies[index].wait()
        out_ref[:, index * piece : (index + 1) * piece] = (
            own + landed[index].astype(jnp.float32)
        ).astype(jnp.bfloat16)


def merge(attended, swished, att_gain, conv_gain, att_w, conv_w):
    rows = attended.shape[0]
    width = att_w.shape[1] // 2
    pieces = 4
    vmem = pl.BlockSpec(memory_space=pltpu.VMEM)
    return pl.pallas_call(
        output_kernel,
        out_shape=jax.ShapeDtypeStruct((rows, width), jnp.bfloat16),
        in_specs=[vmem] * 4 + [pl.BlockSpec(memory_space=pltpu.HBM)] * 2,
        out_specs=vmem,
        scratch_shapes=[
            pltpu.VMEM(att_w.shape, jnp.bfloat16),
            pltpu.VMEM(conv_w.shape, jnp.bfloat16),
            pltpu.VMEM((rows, 256), jnp.float32),
            pltpu.VMEM((rows, 256), jnp.float32),
            pltpu.VMEM((pieces, rows, width // pieces), jnp.bfloat16),
            pltpu.VMEM((pieces, rows, width // pieces), jnp.bfloat16),
            pltpu.SemaphoreType.DMA((2,)),
            pltpu.SemaphoreType.DMA,
            pltpu.SemaphoreType.DMA,
            pltpu.SemaphoreType.DMA((pieces,)),
            pltpu.SemaphoreType.DMA((pieces,)),
        ],
        compiler_params=pltpu.CompilerParams(collective_id=1, has_side_effects=True),
        name="output_merge",
    )(attended, swished, att_gain, conv_gain, att_w, conv_w)


PLANE = 4


def attention_kernel(
    q_ref, own_ref, kup_ref, vup_ref, o_ref, kt, vt, run_max, acc, lat_ref,
    col_send, plane_send, core_send, link_recv, core_recv,
):
    heads, rows, lanes = q_ref.shape
    blocks = lat_ref.shape[0]
    rank = kup_ref.shape[1]
    nope = kup_ref.shape[0] // heads
    vdim = vup_ref.shape[0] // heads
    rot = lat_ref.shape[1] - rank
    wide = kt.shape[2]
    pairing = wide // rows
    me = lax.axis_index("sp")
    core = lax.axis_index("tp")
    layers = blocks // PLANE
    layer = me // PLANE
    spot = me % PLANE
    height = lat_ref.shape[1] // 2
    half = pl.ds(pl.multiple_of(core * height, 16), height)

    def spot_at(distance):
        return (spot + distance) % PLANE

    def at(layer_id, spot_id):
        return {"sp": layer_id * PLANE + spot_id, "tp": core}

    greet(
        [at((layer + d) % layers, spot) for d in range(1, layers)]
        + [at(layer, spot_at(d)) for d in range(1, PLANE)]
        + [other_core()]
    )

    def column_copy(distance):
        return push(
            own_ref.at[half],
            lat_ref.at[me, half],
            col_send.at[distance - 1],
            link_recv.at[me],
            at(jnp.minimum(layer + distance, layers - 1), spot),
        )

    def plane_copy(source, block, distance):
        return push(
            source,
            lat_ref.at[block, half],
            plane_send.at[block // PLANE, distance - 1],
            link_recv.at[block],
            at(layer, spot_at(distance)),
        )

    def core_copy(block):
        spread = lat_ref.at[block, half]
        return push(spread, spread, core_send.at[block], core_recv.at[block], other_core())

    for d in range(1, PLANE):
        plane_copy(own_ref.at[half], me, d).start()
    for d in range(1, layers):

        @pl.when(layer + d < layers)
        def _(d=d):
            column_copy(d).start()

    lat_ref[me] = own_ref[...]

    def relay(step):
        @pl.when(step <= layer)
        def _():
            block = (layer - step) * PLANE + spot
            landed(block)
            for d in range(1, PLANE):
                plane_copy(lat_ref.at[block, half], block, d).start()
            core_copy(block).start()

    def hand_over(step):
        @pl.when(step <= layer)
        def _():
            for d in range(1, PLANE):
                block = (layer - step) * PLANE + spot_at(d)
                landed(block)
                core_copy(block).start()

    def landed(block):
        spread = lat_ref.at[block, half]
        push(spread, spread, core_send.at[block], link_recv.at[block], other_core()).wait_recv()

    def gathered(step):
        for d in range(1, PLANE):
            core_copy((layer - step) * PLANE + spot_at(d)).wait_recv()

    def expand(pair):
        for part in range(pairing):
            src = pair * pairing + part
            lat = lat_ref[src, :rank, :]
            turned = lat_ref[src, rank:, :]
            cols = slice(part * rows, (part + 1) * rows)
            keys = jnp.dot(kup_ref[...], lat, preferred_element_type=jnp.float32)
            values = jnp.dot(vup_ref[...], lat, preferred_element_type=jnp.float32)
            for head in range(heads):
                kt[head, :nope, cols] = keys[head * nope : (head + 1) * nope].astype(jnp.bfloat16)
                kt[head, nope : nope + rot, cols] = turned
                vt[head, :vdim, cols] = values[head * vdim : (head + 1) * vdim].astype(
                    jnp.bfloat16
                )

    def score(head):
        return jnp.dot(q_ref[head], kt[head], preferred_element_type=jnp.float32)

    def weigh(head, scores, top):
        weights = jnp.exp2(scores - top).astype(jnp.bfloat16)
        return lax.dot_general(
            weights, vt[head], (((1,), (1,)), ((), ())), preferred_element_type=jnp.float32
        )

    def visit(group, middle):
        expand(group)
        ahead = score(0)
        for head in range(heads):
            if head == heads // 2:
                middle()
            scores = ahead
            if head + 1 < heads:
                ahead = score(head + 1)
            old = run_max[head]
            top = jnp.maximum(old[:, :1], jnp.max(scores, axis=1, keepdims=True))
            wide_top = jnp.broadcast_to(top, (rows, lanes))
            run_max[head] = wide_top
            acc[head] = acc[head] * jnp.exp2(old - wide_top) + weigh(head, scores, top)

    kt[:, nope + rot :, :] = jnp.zeros((heads, lanes - nope - rot, wide), jnp.bfloat16)
    vt[:, vdim:, :] = jnp.ones((heads, lanes - vdim, wide), jnp.bfloat16)
    hand_over(0)
    relay(1)
    gathered(0)
    expand(layer)
    key_pos = layer * wide + lax.broadcasted_iota(jnp.int32, (rows, wide), 1)
    query_pos = me * rows + lax.broadcasted_iota(jnp.int32, (rows, wide), 0)
    hidden = key_pos > query_pos
    ahead = score(0)
    for head in range(heads):
        if head == heads // 2:
            hand_over(1)
            relay(2)
        scores = jnp.where(hidden, far_below, ahead)
        if head + 1 < heads:
            ahead = score(head + 1)
        top = jnp.max(scores, axis=1, keepdims=True)
        run_max[head] = jnp.broadcast_to(top, (rows, lanes))
        acc[head] = weigh(head, scores, top)

    def far(step, carry):
        for d in range(PLANE):
            core_copy((layer - step) * PLANE + spot_at(d)).wait_recv()

        def middle():
            hand_over(step + 1)
            relay(step + 2)

        visit(layer - step, middle)
        return carry

    lax.fori_loop(1, layer + 1, far, 0)
    lane = lax.broadcasted_iota(jnp.int32, (rows, lanes), 1)
    for pair in range(heads // 2):
        halves = []
        for head in (2 * pair, 2 * pair + 1):
            total = acc[head]
            halves.append(total / pltpu.roll(total, vdim, axis=1))
        both = jnp.where(lane < vdim, halves[0], pltpu.roll(halves[1], vdim, axis=1))
        o_ref[:, pair * lanes : (pair + 1) * lanes] = both.astype(jnp.bfloat16)

    for d in range(1, layers):

        @pl.when(layer + d < layers)
        def _(d=d):
            column_copy(d).wait_send()

    def settle(step, carry):
        base = (layer - step) * PLANE
        for d in range(1, PLANE):
            plane_copy(own_ref.at[half], base + spot, d).wait_send()
            core_copy(base + spot_at(d)).wait_send()

        @pl.when(step > 0)
        def _():
            core_copy(base + spot).wait_send()

        return carry

    lax.fori_loop(0, layer + 1, settle, 0)


def attention(q_heads, packed, key_up_t, value_up_t):
    heads, rows, lanes = q_heads.shape
    blocks = lax.axis_size("sp")
    wide = PLANE * rows
    layers = blocks // PLANE
    vmem = pl.BlockSpec(memory_space=pltpu.VMEM)
    dma = pltpu.SemaphoreType.DMA
    return pl.pallas_call(
        attention_kernel,
        out_shape=jax.ShapeDtypeStruct((rows, value_up_t.shape[0]), jnp.bfloat16),
        in_specs=[vmem] * 4,
        out_specs=vmem,
        scratch_shapes=[
            pltpu.VMEM((heads, lanes, wide), jnp.bfloat16),
            pltpu.VMEM((heads, lanes, wide), jnp.bfloat16),
            pltpu.VMEM((heads, rows, lanes), jnp.float32),
            pltpu.VMEM((heads, rows, lanes), jnp.float32),
            pltpu.VMEM((blocks,) + packed.shape, jnp.bfloat16),
            dma((max(layers - 1, 1),)),
            dma((layers, PLANE - 1)),
            dma((blocks,)),
            dma((blocks,)),
            dma((blocks,)),
        ],
        compiler_params=pltpu.CompilerParams(
            vmem_limit_bytes=40 << 20, collective_id=2, has_side_effects=True
        ),
        name="attention",
    )(q_heads, packed, key_up_t, value_up_t)


def gathered_kernel(q_ref, lat_ref, kup_ref, vup_ref, o_ref, kt, vt, run_max, acc):
    heads, rows, lanes = q_ref.shape
    blocks = lat_ref.shape[0]
    rank = kup_ref.shape[1]
    nope = kup_ref.shape[0] // heads
    vdim = vup_ref.shape[0] // heads
    rot = lat_ref.shape[1] - rank
    wide = kt.shape[2]
    group = wide // rows
    me = lax.axis_index("sp")
    last = me // group
    kt[:, nope + rot :, :] = jnp.zeros((heads, lanes - nope - rot, wide), jnp.bfloat16)
    vt[:, vdim:, :] = jnp.ones((heads, lanes - vdim, wide), jnp.bfloat16)

    def expand(block):
        for part in range(group):
            src = jnp.minimum(block * group + part, blocks - 1)
            lat = lat_ref[src, :rank, :]
            turned = lat_ref[src, rank:, :]
            cols = slice(part * rows, (part + 1) * rows)
            keys = jnp.dot(kup_ref[...], lat, preferred_element_type=jnp.float32)
            values = jnp.dot(vup_ref[...], lat, preferred_element_type=jnp.float32)
            for head in range(heads):
                kt[head, :nope, cols] = keys[head * nope : (head + 1) * nope].astype(jnp.bfloat16)
                kt[head, nope : nope + rot, cols] = turned
                vt[head, :vdim, cols] = values[head * vdim : (head + 1) * vdim].astype(
                    jnp.bfloat16
                )

    def weigh(head, scores, top):
        weights = jnp.exp2(scores - top).astype(jnp.bfloat16)
        return lax.dot_general(
            weights, vt[head], (((1,), (1,)), ((), ())), preferred_element_type=jnp.float32
        )

    expand(last)
    key_pos = last * wide + lax.broadcasted_iota(jnp.int32, (rows, wide), 1)
    query_pos = me * rows + lax.broadcasted_iota(jnp.int32, (rows, wide), 0)
    hidden = key_pos > query_pos
    for head in range(heads):
        scores = jnp.dot(q_ref[head], kt[head], preferred_element_type=jnp.float32)
        scores = jnp.where(hidden, far_below, scores)
        top = jnp.max(scores, axis=1, keepdims=True)
        run_max[head] = jnp.broadcast_to(top, (rows, lanes))
        acc[head] = weigh(head, scores, top)

    def visit(step, carry):
        expand(step)
        for head in range(heads):
            scores = jnp.dot(q_ref[head], kt[head], preferred_element_type=jnp.float32)
            old = run_max[head]
            top = jnp.maximum(old[:, :1], jnp.max(scores, axis=1, keepdims=True))
            wide_top = jnp.broadcast_to(top, (rows, lanes))
            run_max[head] = wide_top
            acc[head] = acc[head] * jnp.exp2(old - wide_top) + weigh(head, scores, top)
        return carry

    lax.fori_loop(0, last, visit, 0)
    lane = lax.broadcasted_iota(jnp.int32, (rows, lanes), 1)
    for pair in range(heads // 2):
        halves = []
        for head in (2 * pair, 2 * pair + 1):
            total = acc[head]
            halves.append(total / pltpu.roll(total, vdim, axis=1))
        both = jnp.where(lane < vdim, halves[0], pltpu.roll(halves[1], vdim, axis=1))
        o_ref[:, pair * lanes : (pair + 1) * lanes] = both.astype(jnp.bfloat16)


def gathered_attention(q_heads, lat_all, key_up_t, value_up_t):
    heads, rows, lanes = q_heads.shape
    blocks = lat_all.shape[0]
    wide = 2 * rows if blocks % 2 == 0 else rows
    vmem = pl.BlockSpec(memory_space=pltpu.VMEM)
    return pl.pallas_call(
        gathered_kernel,
        out_shape=jax.ShapeDtypeStruct((rows, value_up_t.shape[0]), jnp.bfloat16),
        in_specs=[vmem] * 4,
        out_specs=vmem,
        scratch_shapes=[
            pltpu.VMEM((heads, lanes, wide), jnp.bfloat16),
            pltpu.VMEM((heads, lanes, wide), jnp.bfloat16),
            pltpu.VMEM((heads, rows, lanes), jnp.float32),
            pltpu.VMEM((heads, rows, lanes), jnp.float32),
        ],
        compiler_params=pltpu.CompilerParams(vmem_limit_bytes=48 << 20),
        cost_estimate=pl.CostEstimate(
            flops=20_000_000_000, bytes_accessed=8 << 20, transcendentals=20_000_000
        ),
        name="gathered_attention",
    )(q_heads, lat_all, key_up_t, value_up_t)


def conv_kernel(gated_ref, rim_ref, taps_ref, out_ref, wide):
    rows, chans = gated_ref.shape
    rim = rim_ref.shape[0]
    taps = taps_ref.shape[0]
    chunk = 64
    for part in range(chans // 128):
        cols = slice(part * 128, (part + 1) * 128)
        wide[part, :rim, :] = rim_ref[:, cols].astype(jnp.float32)
        wide[part, rim:, :] = gated_ref[:, cols].astype(jnp.float32)
        coeff = taps_ref[:, cols]

        def band(step, carry):
            base = step * chunk
            total = jnp.zeros((chunk, 128), jnp.float32)
            for tap in range(taps):
                total = total + coeff[tap : tap + 1, :] * wide[
                    part, pl.ds(base + (rim - taps + 1 + tap), chunk), :
                ]
            out_ref[pl.ds(pl.multiple_of(base, chunk), chunk), cols] = total
            return carry

        lax.fori_loop(0, rows // chunk, band, 0)


def convolve(gated, rim, taps):
    rows, chans = gated.shape
    vmem = pl.BlockSpec(memory_space=pltpu.VMEM)
    return pl.pallas_call(
        conv_kernel,
        out_shape=jax.ShapeDtypeStruct((rows, chans), jnp.float32),
        in_specs=[vmem] * 3,
        out_specs=vmem,
        scratch_shapes=[pltpu.VMEM((chans // 128, rows + rim.shape[0], 128), jnp.float32)],
        cost_estimate=pl.CostEstimate(
            flops=2 * rows * chans * 31, bytes_accessed=2 << 20, transcendentals=0
        ),
        name="depthwise",
    )(gated, rim, taps)


def shards(
    tokens,
    input_gain,
    query_weight,
    query_rot_weight,
    kv_down,
    rot_down,
    kv_gain,
    key_up,
    value_up,
    conv_value_weight,
    conv_gate_weight,
    conv_taps,
    conv_ln_gain,
    conv_ln_bias,
    att_out_gain,
    conv_out_gain,
    att_out_weight,
    conv_out_weight,
):
    tok_rows = tokens.shape[0]
    heads_here = key_up.shape[1] // NOPE_DIM
    chan_here = conv_taps.shape[1]
    weight_list = (
        query_weight,
        query_rot_weight,
        kv_down,
        rot_down,
        conv_value_weight,
        conv_gate_weight,
    )
    if lax.axis_size("tp") == 2 and lax.axis_size("sp") % PLANE == 0:
        positions = lax.axis_index("sp") * tok_rows + jnp.arange(tok_rows, dtype=jnp.int32)
        cos_table, sine_table = rotary_tables(positions, ROT_DIM // 2)
        q_heads, packed, swished = front(
            tokens,
            input_gain[None, :],
            kv_gain[None, :],
            cos_table.T,
            sine_table.T,
            conv_taps,
            conv_ln_gain[None, :],
            conv_ln_bias[None, :],
            weight_list[:3] + (rot_down.T,) + weight_list[4:],
        )
        attended = attention(q_heads, packed, key_up.T, value_up.T)
        return merge(
            attended,
            swished,
            att_out_gain[None, :],
            conv_out_gain[None, :],
            att_out_weight,
            conv_out_weight,
        )
    whole_rows = lax.all_gather(tokens, "tp", axis=1, tiled=True).astype(jnp.float32)
    scaled = (whole_rows * input_gain[None, :]).astype(jnp.bfloat16)
    row_scale = lax.rsqrt(jnp.mean(whole_rows * whole_rows, axis=1, keepdims=True) + norm_eps)

    def add_product(weight):
        return jnp.dot(scaled, weight, preferred_element_type=jnp.float32)

    summed = tuple((add_product(weight) for weight in weight_list))
    q_acc, qrot_acc, latent_raw, rot_acc, value_acc, gate_acc = summed
    positions = lax.axis_index("sp") * tok_rows + jnp.arange(tok_rows, dtype=jnp.int32)
    cos_table, sine_table = rotary_tables(positions, ROT_DIM // 2)
    fold = math.log2(math.e) / math.sqrt(NOPE_DIM + ROT_DIM)
    query_scale = row_scale * fold
    plain_q = (q_acc * query_scale).reshape(tok_rows, heads_here, NOPE_DIM)
    turned_q = rotate_half(
        (qrot_acc * query_scale).reshape(tok_rows, heads_here, ROT_DIM),
        cos_table[:, None, :],
        sine_table[:, None, :],
    )
    blank = jnp.zeros((tok_rows, heads_here, 128 - NOPE_DIM - ROT_DIM), jnp.float32)
    q_heads = jnp.transpose(
        jnp.concatenate([plain_q, turned_q, blank], axis=2).astype(jnp.bfloat16), (1, 0, 2)
    )
    latent = (
        latent_raw
        * lax.rsqrt(jnp.mean(latent_raw * latent_raw, axis=1, keepdims=True) + norm_eps)
        * kv_gain[None, :]
    ).astype(jnp.bfloat16)
    key_rot = rotate_half(rot_acc * row_scale, cos_table, sine_table).astype(jnp.bfloat16)
    gated_input = (value_acc * row_scale * jax.nn.sigmoid(gate_acc * row_scale)).astype(
        jnp.bfloat16
    )
    packed = jnp.concatenate([latent.T, key_rot.T], axis=0)
    rim_rows = shifted(gated_input[tok_rows - (KERNEL + 1) :], "sp", 1)
    conv_out = convolve(gated_input, rim_rows, conv_taps)
    moment_one, moment_two = lax.psum(
        (jnp.sum(conv_out, axis=1), jnp.sum(conv_out * conv_out, axis=1)), "tp"
    )
    mean_val = moment_one / CONV_CH
    spread = moment_two / CONV_CH - mean_val * mean_val
    normed = (conv_out - mean_val[:, None]) * lax.rsqrt(spread + norm_eps)[:, None]
    swished = jax.nn.silu(normed * conv_ln_gain[None, :] + conv_ln_bias[None, :])
    lat_all = lax.all_gather(packed, "sp", axis=0)
    attended = gathered_attention(q_heads, lat_all, key_up.T, value_up.T).astype(jnp.float32)
    att_sq, conv_sq = lax.psum(
        (
            jnp.sum(attended * attended, axis=1, keepdims=True),
            jnp.sum(swished * swished, axis=1, keepdims=True),
        ),
        "tp",
    )
    att_mixed = (
        attended * lax.rsqrt(att_sq / ATT_WIDTH + norm_eps) * att_out_gain[None, :]
    ).astype(jnp.bfloat16)
    conv_mixed = (
        swished * lax.rsqrt(conv_sq / CONV_CH + norm_eps) * conv_out_gain[None, :]
    ).astype(jnp.bfloat16)
    share = (
        jnp.dot(att_mixed, att_out_weight, preferred_element_type=jnp.float32)
        + jnp.dot(conv_mixed, conv_out_weight, preferred_element_type=jnp.float32)
    ).astype(jnp.bfloat16)
    return lax.psum_scatter(share, "tp", scatter_dimension=1, tiled=True)


def solution(mesh):
    return jax.shard_map(
        shards,
        mesh=mesh,
        in_specs=(
            P("sp", "tp"),
            P(),
            P(None, "tp"),
            P(None, "tp"),
            P(),
            P(),
            P(),
            P(None, "tp"),
            P(None, "tp"),
            P(None, "tp"),
            P(None, "tp"),
            P(None, "tp"),
            P("tp"),
            P("tp"),
            P("tp"),
            P("tp"),
            P("tp", None),
            P("tp", None),
        ),
        out_specs=P("sp", "tp"),
        check_vma=False,
    )
```

profile of v0, /device:TPU:25, one launch (start us, length us, event | category | flops | bytes accessed | tf_op | source)
XLA Modules:
  0.0 76.3 jit_solution(8317202703856731021)
XLA Ops:
  0.0 0.8 %multiply_sine_fusion = (f32[16,384]{1,0:T(8,128)}, f32[16,384]{1,0:T(8,128)}) fusion(f32[16]{0:T(128)S(1)} %multiply_power_fusion, f32[384]{0:T(512)S(1)} %add_convert_fusion), kind=kLoop, calls=%fused_computation | loop fusion | flops 6144 | bytes 50752 | tf_op jit(solution)/shard_map/sin | solution.py:33
  0.8 1.1 %copy.19 = bf16[256,512]{0,1:T(8,128)(2,1)S(1)} copy(bf16[256,512]{1,0:T(8,128)(2,1)} %param.25) | data formatting | bytes 524288 | tf_op args[7]
  1.9 1.1 %copy.20 = bf16[256,512]{0,1:T(8,128)(2,1)S(1)} copy(bf16[256,512]{1,0:T(8,128)(2,1)} %param.26) | data formatting | bytes 524288 | tf_op args[8]
  3.0 17.2 %front.1 = (bf16[8,384,128]{2,1,0:T(8,128)(2,1)}, bf16[288,384]{1,0:T(8,128)(2,1)}, f32[384,512]{1,0:T(8,128)}) custom-call(bf16[384,1024]{1,0:T(8,128)(2,1)} %tok_ref.1, f32[1,2048]{1,0:T(1,128)} %bitcast.12, f32[1,256]{1,0:T(1,128)} %bitcast.17, f32[16,384]{1,0:T(8,128)} %get-tuple-element.12.cos_ref, f32[16,384]{1,0:T(8,128)} %get-tuple-element.11.sin_ref, ...), custom_call_target="tpu_custom_call" | custom-call | tf_op jit(solution)/shard_map/front/pallas_call | solution.py:227
  20.2 0.0 copy-start.1
  20.2 1.1 %copy-done.1 = bf16[8,384,128]{2,1,0:T(8,128)(2,1)S(1)} copy-done((bf16[8,384,128]{2,1,0:T(8,128)(2,1)S(1)}, bf16[8,384,128]{2,1,0:T(8,128)(2,1)}, u32[]{:S(2)}) %copy-start.1) | copy-done | bytes 786456
  21.4 0.0 copy-start.2
  21.4 0.9 %copy-done.2 = bf16[288,384]{1,0:T(8,128)(2,1)S(1)} copy-done((bf16[288,384]{1,0:T(8,128)(2,1)S(1)}, bf16[288,384]{1,0:T(8,128)(2,1)}, u32[]{:S(2)}) %copy-start.2) | copy-done | bytes 221208
  22.3 41.9 %attention.1.att_ref = bf16[384,512]{1,0:T(8,128)(2,1)S(1)} custom-call(bf16[8,384,128]{2,1,0:T(8,128)(2,1)S(1)} %copy-done.1, bf16[288,384]{1,0:T(8,128)(2,1)S(1)} %copy-done.2, bf16[512,256]{1,0:T(8,128)(2,1)S(1)} %bitcast.9, bf16[512,256]{1,0:T(8,128)(2,1)S(1)} %bitcast.10), custom_call_target="tpu_custom_call" | custom-call | tf_op jit(solution)/shard_map/attention/pallas_call | solution.py:541
  64.2 0.0 copy-start
  64.3 0.7 copy-done
  65.0 9.2 %output_merge.1 = bf16[384,1024]{1,0:T(8,128)(2,1)} custom-call(bf16[384,512]{1,0:T(8,128)(2,1)} %copy-done, f32[384,512]{1,0:T(8,128)} %get-tuple-element.10.swish_ref, f32[1,512]{1,0:T(1,128)} %bitcast.13, f32[1,512]{1,0:T(1,128)} %bitcast.14, bf16[512,2048]{1,0:T(8,128)(2,1)} %att_hbm.1, bf16[512,2048]{1,0:T(8,128)(2,1)} %conv_hbm.1), custom_call_target="tpu_custom_call" | custom-call | tf_op jit(solution)/shard_map/output_merge/pallas_call | solution.py:317
  74.2 2.1 %copy.22 = bf16[384,1024]{1,0:T(8,128)(2,1)} copy(bf16[384,1024]{1,0:T(8,128)(2,1)} %output_merge.1) | data formatting | bytes 1572864
  (2 shorter events, 0.0 us)
Async XLA Ops:
  20.2 1.1 %copy-start.1 = (bf16[8,384,128]{2,1,0:T(8,128)(2,1)S(1)}, bf16[8,384,128]{2,1,0:T(8,128)(2,1)}, u32[]{:S(2)}) copy-start(bf16[8,384,128]{2,1,0:T(8,128)(2,1)} %get-tuple-element.8.q_ref) | copy-start | bytes 2359300
  21.4 0.9 %copy-start.2 = (bf16[288,384]{1,0:T(8,128)(2,1)S(1)}, bf16[288,384]{1,0:T(8,128)(2,1)}, u32[]{:S(2)}) copy-start(bf16[288,384]{1,0:T(8,128)(2,1)} %get-tuple-element.9.own_ref) | copy-start | bytes 663556
  64.2 0.7 copy-start
where the time goes:
time: 76.6 us; the launch traced here: 76.3 us
  Pallas kernels  68.4 us (89%)
  local copies, waits for them, and re-layouts  7.03 us (9%)
  other arithmetic  0.8 us (1%)
    pallas_call x1, Pallas kernels, attention(): pl.pallas_call(attention_kernel, out_shape=jax.ShapeDtypeStruct((rows, va...  41.9 us
    pallas_call x1, Pallas kernels, front(): pl.pallas_call(front_kernel, out_shape=(jax.ShapeDtypeStruct((heads, rows...  17.2 us
    pallas_call x1, Pallas kernels, merge(): pl.pallas_call(output_kernel, out_shape=jax.ShapeDtypeStruct((rows, width...  9.21 us
    unnamed x9, local copies, waits for them, and re-layouts  7.03 us

commit v1 on v0

v1 whole, which is shorter than its diff:
```python
import math

import jax
import jax.numpy as jnp
import numpy as np
from jax import lax
from jax.experimental import pallas as pl
from jax.experimental.pallas import tpu as pltpu
from jax.sharding import PartitionSpec as P

D_MODEL = 2048
NOPE_DIM = 64
ROT_DIM = 32
VALUE_DIM = 64
CONV_CH = 1024
KERNEL = 31
ATT_WIDTH = 1024


norm_eps = 1e-06
far_below = -1e30
rope_base = 10000.0


def shifted(block, axis, distance):
    devices = range(lax.axis_size(axis))
    route = [(i - distance, i) for i in devices if i - distance in devices]
    return lax.ppermute(block, axis, route)


def rotary_tables(positions, half_dim):
    frequency = rope_base ** (-jnp.arange(half_dim, dtype=jnp.float32) / half_dim)
    angles = positions.astype(jnp.float32)[:, None] * frequency[None, :]
    return (jnp.cos(angles), jnp.sin(angles))


def rotate_half(values, cos_table, sine_table):
    half_dim = cos_table.shape[-1]
    front_half = values[..., :half_dim]
    back_half = values[..., half_dim:]
    return jnp.concatenate(
        [
            front_half * cos_table - back_half * sine_table,
            back_half * cos_table + front_half * sine_table,
        ],
        axis=-1,
    )


MESH = pl.DeviceIdType.MESH


def push(src, dst, send, recv, target):
    return pltpu.make_async_remote_copy(
        src_ref=src,
        dst_ref=dst,
        send_sem=send,
        recv_sem=recv,
        device_id=target,
        device_id_type=MESH,
    )


def other_core():
    return {"sp": lax.axis_index("sp"), "tp": 1 - lax.axis_index("tp")}


PLANE = 4


def layer_kernel(
    tok_hbm, gain_ref, kv_gain_ref, base_ref, seat_ref, taps_ref, ln_gain_ref, ln_bias_ref,
    att_gain_ref, conv_gain_ref,
    kvd_hbm, rotw_hbm, cgw_hbm, cvw_hbm, qw_hbm, qrw_hbm, kup_hbm, vup_hbm, att_hbm, conv_hbm,
    out_ref,
    kvd, rotw, cgw, cvw, qw, qrw, kup, vup, att_w, conv_w, vup_t,
    tok, landed, scaled, narrow, gated, rim, wide, conv, sq_mine, sq_other,
    lat_ref, q2, kn, kr, vt, run_max, acc, s_ref, att_t, end_mine, end_other, part, arrived,
    w_sem, tok_load, tok_send, tok_recv, rim_send, rim_recv, sq_send, sq_recv,
    csq_send, csq_recv, asq_send, asq_recv, part_send, part_recv,
    col_send, plane_send, core_send, link_recv, core_recv,
):
    mine = lax.axis_index("tp")
    me = lax.axis_index("sp")
    seats = lax.axis_size("sp")
    rows, width = tok.shape
    blocks = lat_ref.shape[0]
    rank = kvd.shape[1]
    layers = blocks // PLANE
    layer = me // PLANE
    spot = me % PLANE
    height = lat_ref.shape[1] // 2
    half = pl.ds(pl.multiple_of(mine * height, 16), height)
    other = other_core()
    ahead = {"sp": (me + 1) % seats, "tp": mine}
    behind = {"sp": (me + seats - 1) % seats, "tp": mine}

    loads = [
        pltpu.make_async_copy(src, dst, w_sem.at[index])
        for index, (src, dst) in enumerate(
            (
                (kvd_hbm, kvd), (rotw_hbm, rotw), (cgw_hbm, cgw), (cvw_hbm, cvw),
                (qw_hbm, qw), (qrw_hbm, qrw), (kup_hbm, kup), (vup_hbm, vup),
                (att_hbm, att_w), (conv_hbm, conv_w),
            )
        )
    ]
    fetch = pltpu.make_async_copy(tok_hbm, tok, tok_load)
    fetch.start()
    for load in loads:
        load.start()

    def spot_at(distance):
        return (spot + distance) % PLANE

    def at(layer_id, spot_id):
        return {"sp": layer_id * PLANE + spot_id, "tp": mine}

    barrier = pltpu.get_barrier_semaphore()
    peers = (
        [at((layer + d) % layers, spot) for d in range(1, layers)]
        + [at(layer, spot_at(d)) for d in range(1, PLANE)]
        + [other]
    )
    for peer in peers:
        pl.semaphore_signal(barrier, inc=1, device_id=peer, device_id_type=MESH)

    @pl.when(me < seats - 1)
    def _():
        pl.semaphore_signal(barrier, inc=1, device_id=ahead, device_id_type=MESH)

    @pl.when(me > 0)
    def _():
        pl.semaphore_signal(barrier, inc=1, device_id=behind, device_id_type=MESH)

    q2[...] = jnp.zeros(q2.shape, jnp.bfloat16)
    pairs, _, both = q2.shape
    keys_wide = kn.shape[0]
    ones_low = VALUE_DIM
    ones_high = vt.shape[1] - VALUE_DIM
    vt[:, ones_low:ones_high, :] = jnp.ones((pairs, ones_high - ones_low, keys_wide), jnp.bfloat16)
    pl.semaphore_wait(
        barrier, len(peers) + jnp.minimum(me, 1) + jnp.minimum(seats - 1 - me, 1)
    )
    fetch.wait()
    tok_copy = push(tok, landed, tok_send, tok_recv, other)
    tok_copy.start()

    def place(block, index):
        cols = pl.ds(pl.multiple_of(index * width, 128), width)
        full = block[...].astype(jnp.float32)
        scaled[:, cols] = (full * gain_ref[:, cols]).astype(jnp.bfloat16)
        return jnp.sum(full * full, axis=1, keepdims=True)

    squares = place(tok, mine)
    loads[7].wait()
    vup_t[...] = vup[...].astype(jnp.float32).T.astype(jnp.bfloat16)
    column = lax.broadcasted_iota(jnp.int32, seat_ref.shape, 1)
    seat_turn = jnp.sum(
        jnp.where(column == me, seat_ref[...], 0.0), axis=1, keepdims=True
    )
    turn = ROT_DIM // 2
    seat_cos, seat_sin = seat_turn[:turn], seat_turn[turn:]
    base_cos, base_sin = base_ref[:turn], base_ref[turn:]
    cos_table = seat_cos * base_cos - seat_sin * base_sin
    sin_table = seat_sin * base_cos + seat_cos * base_sin

    def rotate(block):
        front = block[:turn]
        back = block[turn : 2 * turn]
        return jnp.concatenate(
            [front * cos_table - back * sin_table, back * cos_table + front * sin_table], axis=0
        )

    tok_copy.wait()
    squares = squares + place(landed, 1 - mine)
    row_scale = lax.rsqrt(squares / (2 * width) + norm_eps)

    def project(weight):
        return jnp.dot(scaled[...], weight[...], preferred_element_type=jnp.float32)

    loads[0].wait()
    loads[1].wait()
    raw = project(kvd)
    latent = (
        raw
        * lax.rsqrt(jnp.mean(raw * raw, axis=1, keepdims=True) + norm_eps)
        * kv_gain_ref[...]
    )
    lat_ref[me, :rows, :] = latent.astype(jnp.bfloat16)
    narrow[...] = jnp.broadcast_to(row_scale, narrow.shape)
    key_turn = lax.dot_general(
        rotw[...], scaled[...], (((1,), (1,)), ((), ())), preferred_element_type=jnp.float32
    )
    key_rot = rotate(key_turn * narrow[...].T[:ROT_DIM]).astype(jnp.bfloat16)
    across = rank // 128
    for piece in range(across * ((rows // 128 + across - 1) // across)):
        band = rows + piece // across * ROT_DIM
        lanes = slice(piece % across * 128, piece % across * 128 + 128)
        lat_ref[me, band : band + ROT_DIM, lanes] = (
            key_rot[:, piece * 128 : piece * 128 + 128]
            if piece < rows // 128
            else jnp.zeros((ROT_DIM, 128), jnp.bfloat16)
        )

    def column_copy(distance):
        return push(
            lat_ref.at[me, half],
            lat_ref.at[me, half],
            col_send.at[distance - 1],
            link_recv.at[me],
            at(jnp.minimum(layer + distance, layers - 1), spot),
        )

    def plane_copy(block, distance):
        return push(
            lat_ref.at[block, half],
            lat_ref.at[block, half],
            plane_send.at[block // PLANE, distance - 1],
            link_recv.at[block],
            at(layer, spot_at(distance)),
        )

    def core_copy(block):
        spread = lat_ref.at[block, half]
        return push(spread, spread, core_send.at[block], core_recv.at[block], other)

    for d in range(1, PLANE):
        plane_copy(me, d).start()
    for d in range(1, layers):

        @pl.when(layer + d < layers)
        def _(d=d):
            column_copy(d).start()

    def arrive(block):
        spread = lat_ref.at[block, half]
        push(spread, spread, core_send.at[block], link_recv.at[block], other).wait_recv()

    def relay(step):
        @pl.when(step <= layer)
        def _():
            block = (layer - step) * PLANE + spot
            arrive(block)
            for d in range(1, PLANE):
                plane_copy(block, d).start()
            core_copy(block).start()

    def hand_over(step):
        @pl.when(step <= layer)
        def _():
            for d in range(1, PLANE):
                block = (layer - step) * PLANE + spot_at(d)
                arrive(block)
                core_copy(block).start()

    loads[2].wait()
    loads[3].wait()
    gate = project(cgw) * row_scale
    gated[...] = (project(cvw) * row_scale * jax.nn.sigmoid(gate)).astype(jnp.bfloat16)
    edge = rim.shape[0]
    rim_copy = push(gated.at[pl.ds(rows - edge, edge)], rim, rim_send, rim_recv, ahead)

    @pl.when(me < seats - 1)
    def _():
        rim_copy.start()

    loads[4].wait()
    loads[5].wait()
    query_scale = row_scale * (math.log2(math.e) / math.sqrt(NOPE_DIM + ROT_DIM))
    plain = (project(qw) * query_scale).T.astype(jnp.bfloat16)
    turned = (project(qrw) * query_scale).T
    for head in range(2 * pairs):
        side = head % 2
        cols = slice(side * rows, (side + 1) * rows)
        q2[head // 2, side * NOPE_DIM : (side + 1) * NOPE_DIM, cols] = plain[
            head * NOPE_DIM : (head + 1) * NOPE_DIM
        ]
        q2[head // 2, 2 * NOPE_DIM : 2 * NOPE_DIM + ROT_DIM, cols] = rotate(
            turned[head * ROT_DIM : (head + 1) * ROT_DIM]
        ).astype(jnp.bfloat16)

    relay(1)

    @pl.when(me > 0)
    def _():
        rim_copy.wait_recv()

    @pl.when(me == 0)
    def _():
        rim[...] = jnp.zeros(rim.shape, jnp.bfloat16)

    taps = taps_ref.shape[0]
    chunk = 64
    for slab in range(conv.shape[1] // 128):
        cols = slice(slab * 128, (slab + 1) * 128)
        wide[slab, :edge, :] = rim[:, cols].astype(jnp.float32)
        wide[slab, edge:, :] = gated[:, cols].astype(jnp.float32)
        coeff = taps_ref[:, cols]

        def band_step(step, carry, slab=slab, cols=cols, coeff=coeff):
            base = step * chunk
            total = jnp.zeros((chunk, 128), jnp.float32)
            for tap in range(taps):
                total = total + coeff[tap : tap + 1, :] * wide[
                    slab, pl.ds(base + (edge - taps + 1 + tap), chunk), :
                ]
            conv[pl.ds(pl.multiple_of(base, chunk), chunk), cols] = total
            return carry

        lax.fori_loop(0, rows // chunk, band_step, 0)

    values = conv[...]
    for slot, total in enumerate((values, values * values)):
        sq_mine[:, slot * 128 : (slot + 1) * 128] = jnp.broadcast_to(
            jnp.sum(total, axis=1, keepdims=True), (rows, 128)
        )
    sums = push(sq_mine, sq_other, sq_send, sq_recv, other)
    sums.start()
    hand_over(0)
    sums.wait()
    moments = (sq_mine[...] + sq_other[...]) / CONV_CH
    mean_val = moments[:, :1]
    spread_val = moments[:, 128:129] - mean_val * mean_val
    normed = (values - mean_val) * lax.rsqrt(spread_val + norm_eps)
    swished = jax.nn.silu(normed * ln_gain_ref[...] + ln_bias_ref[...])
    conv[...] = swished
    end_mine[0] = jnp.broadcast_to(
        jnp.sum(swished * swished, axis=1, keepdims=True), (rows, 128)
    )
    conv_sum = push(end_mine.at[0], end_other.at[0], csq_send, csq_recv, other)
    conv_sum.start()
    relay(2)

    def gathered(step):
        for d in range(1, PLANE):
            core_copy((layer - step) * PLANE + spot_at(d)).wait_recv()

    span = 2 * rows

    def expand(group):
        for index in range(PLANE // 2):
            blk = group * PLANE + 2 * index
            cols = slice(index * span, (index + 1) * span)
            lat = jnp.concatenate([lat_ref[blk, :rows, :], lat_ref[blk + 1, :rows, :]], axis=0)
            kn[cols, :] = jnp.dot(
                lat, kup[...], preferred_element_type=jnp.float32
            ).astype(jnp.bfloat16)
            values = lax.dot_general(
                vup_t[...], lat, (((1,), (1,)), ((), ())), preferred_element_type=jnp.float32
            ).astype(jnp.bfloat16)
            for pair in range(pairs):
                low = 2 * VALUE_DIM * pair
                vt[pair, :ones_low, cols] = values[low : low + VALUE_DIM]
                vt[pair, ones_high:, cols] = values[low + VALUE_DIM : low + 2 * VALUE_DIM]
            for part_id in range(2):
                pieces = []
                for piece in range(rows // 128):
                    band = rows + piece // across * ROT_DIM
                    lanes = slice(piece % across * 128, piece % across * 128 + 128)
                    pieces.append(lat_ref[blk + part_id, band : band + ROT_DIM, lanes])
                rot = jnp.concatenate(pieces, axis=1).astype(jnp.float32)
                rot = jnp.concatenate(
                    [rot, jnp.zeros((128 - ROT_DIM, rows), jnp.float32)], axis=0
                )
                low = index * span + part_id * rows
                kr[low : low + rows, :] = rot.T.astype(jnp.bfloat16)

    strip = 256
    strips = keys_wide // strip
    tiles = both // 256
    tile_rows = tuple(
        (
            0 if 256 * tile < rows else ones_low,
            ones_high if 256 * (tile + 1) <= rows else vt.shape[1],
        )
        for tile in range(tiles)
    )

    def attend(first, hidden, middle):
        def score(pair, index):
            cut = slice(index * strip, (index + 1) * strip)
            keys = jnp.concatenate([kn[cut, 128 * pair : 128 * pair + 128], kr[cut, :]], axis=1)
            scores = jnp.dot(keys, q2[pair], preferred_element_type=jnp.float32)
            if hidden is not None:
                scores = jnp.where(hidden(index), far_below, scores)
            s_ref[pair % 2, cut, :] = scores
            return jnp.max(scores, axis=0, keepdims=True)

        tops = [score(0, index) for index in range(strips)]
        for pair in range(pairs):
            if pair == pairs // 2:
                middle()
            top = tops[0]
            for value in tops[1:]:
                top = jnp.maximum(top, value)
            if not first:
                old = run_max[pair : pair + 1, :]
                top = jnp.maximum(old, top)
                fade = jnp.exp2(old - top)
            run_max[pair : pair + 1, :] = top
            tops = []
            sums = [None] * tiles
            for index in range(strips):
                cut = slice(index * strip, (index + 1) * strip)
                if pair + 1 < pairs:
                    tops.append(score(pair + 1, index))
                weights = jnp.exp2(s_ref[pair % 2, cut, :] - top).astype(jnp.bfloat16)
                for tile, (low, high) in enumerate(tile_rows):
                    new = jnp.dot(
                        vt[pair, low:high, cut],
                        weights[:, 256 * tile : 256 * (tile + 1)],
                        preferred_element_type=jnp.float32,
                    )
                    sums[tile] = new if sums[tile] is None else sums[tile] + new
            for tile, (low, high) in enumerate(tile_rows):
                new = sums[tile]
                if not first:
                    new = new + acc[pair, tile, : high - low, :] * fade[
                        :, 256 * tile : 256 * (tile + 1)
                    ]
                acc[pair, tile, : high - low, :] = new

    def hidden(index):
        key = layer * keys_wide + index * strip + lax.broadcasted_iota(
            jnp.int32, (strip, both), 0
        )
        query = lax.broadcasted_iota(jnp.int32, (strip, both), 1)
        return key > me * rows + jnp.where(query >= rows, query - rows, query)

    loads[6].wait()
    gathered(0)
    expand(layer)

    def first_middle():
        hand_over(1)

    attend(True, hidden, first_middle)

    def far(step, carry):
        for d in range(PLANE):
            core_copy((layer - step) * PLANE + spot_at(d)).wait_recv()
        expand(layer - step)

        def middle():
            hand_over(step + 1)
            relay(step + 2)

        attend(False, None, middle)
        return carry

    lax.fori_loop(1, layer + 1, far, 0)

    for pair in range(pairs):
        for side in range(2):
            pieces = []
            for tile, (low, high) in enumerate(tile_rows):
                start = max(side * rows, 256 * tile)
                stop = min((side + 1) * rows, 256 * (tile + 1))
                if start >= stop:
                    continue
                total = acc[pair, tile, : high - low, start - 256 * tile : stop - 256 * tile]
                base = 0 if side == 0 else ones_high - low
                pieces.append(
                    total[base : base + VALUE_DIM] / total[ones_low - low : ones_low - low + 1]
                )
            low = (2 * pair + side) * VALUE_DIM
            att_t[low : low + VALUE_DIM, :] = jnp.concatenate(pieces, axis=1)
    attended = att_t[...].T.astype(jnp.bfloat16).astype(jnp.float32)
    end_mine[1] = jnp.broadcast_to(
        jnp.sum(attended * attended, axis=1, keepdims=True), (rows, 128)
    )
    att_sum = push(end_mine.at[1], end_other.at[1], asq_send, asq_recv, other)
    att_sum.start()
    conv_sum.wait()
    conv_scale = lax.rsqrt((end_mine[0] + end_other[0])[:, :1] / CONV_CH + norm_eps)
    conv_mixed = (conv[...] * conv_scale * conv_gain_ref[...]).astype(jnp.bfloat16)
    att_mixed = (attended * att_gain_ref[...]).astype(jnp.bfloat16)
    loads[8].wait()
    loads[9].wait()
    pieces = part.shape[0]
    piece = part.shape[2]

    def products(owner, index):
        cols = pl.ds(pl.multiple_of(owner * width + index * piece, 128), piece)
        return (
            jnp.dot(att_mixed, att_w[:, cols], preferred_element_type=jnp.float32),
            jnp.dot(conv_mixed, conv_w[:, cols], preferred_element_type=jnp.float32),
        )

    waiting = [products(1 - mine, index) for index in range(pieces)]
    att_sum.wait()
    att_scale = lax.rsqrt((end_mine[1] + end_other[1])[:, :1] / ATT_WIDTH + norm_eps)
    copies = []
    for index, (from_att, from_conv) in enumerate(waiting):
        part[index] = (from_att * att_scale + from_conv).astype(jnp.bfloat16)
        copy = push(
            part.at[index], arrived.at[index], part_send.at[index], part_recv.at[index], other
        )
        copy.start()
        copies.append(copy)
    for index in range(pieces):
        from_att, from_conv = products(mine, index)
        own = (from_att * att_scale + from_conv).astype(jnp.bfloat16).astype(jnp.float32)
        copies[index].wait()
        out_ref[:, index * piece : (index + 1) * piece] = (
            own + arrived[index].astype(jnp.float32)
        ).astype(jnp.bfloat16)

    @pl.when(me < seats - 1)
    def _():
        rim_copy.wait_send()

    for d in range(1, layers):

        @pl.when(layer + d < layers)
        def _(d=d):
            column_copy(d).wait_send()

    def settle(step, carry):
        base = (layer - step) * PLANE
        for d in range(1, PLANE):
            plane_copy(base + spot, d).wait_send()
            core_copy(base + spot_at(d)).wait_send()

        @pl.when(step > 0)
        def _():
            core_copy(base + spot).wait_send()

        return carry

    lax.fori_loop(0, layer + 1, settle, 0)


def angle_tables(seats, rows):
    frequency = rope_base ** (-np.arange(ROT_DIM // 2) / (ROT_DIM // 2))

    def table(positions):
        angles = frequency[:, None] * positions[None, :]
        return jnp.asarray(
            np.concatenate([np.cos(angles), np.sin(angles)], axis=0), jnp.float32
        )

    return table(np.arange(rows)), table(rows * np.arange(-(-seats // 128) * 128))


def fused(tokens, gains, matrices, taps, seats):
    rows, width = tokens.shape
    chans = taps.shape[1]
    rank = matrices[0].shape[1]
    heads = matrices[4].shape[1] // NOPE_DIM
    pairs = heads // 2
    keys_wide = PLANE * rows
    layers = seats // PLANE
    across = rank // 128
    height = rows + -(-(rows // 128) // across) * ROT_DIM
    vmem = pl.BlockSpec(memory_space=pltpu.VMEM)
    anywhere = pl.BlockSpec(memory_space=pltpu.HBM)
    dma = pltpu.SemaphoreType.DMA
    edge = 32
    pieces = 4
    bf16 = jnp.bfloat16
    f32 = jnp.float32
    value_rows = 2 * VALUE_DIM + 16
    base, seat = angle_tables(seats, rows)
    input_gain, kv_gain, ln_gain, ln_bias, att_gain, conv_gain = gains
    return pl.pallas_call(
        layer_kernel,
        out_shape=jax.ShapeDtypeStruct((rows, width), bf16),
        in_specs=[anywhere] + [vmem] * 9 + [anywhere] * 10,
        out_specs=vmem,
        scratch_shapes=[pltpu.VMEM(matrix.shape, bf16) for matrix in matrices]
        + [
            pltpu.VMEM(matrices[7].shape[::-1], bf16),
            pltpu.VMEM((rows, width), bf16),
            pltpu.VMEM((rows, width), bf16),
            pltpu.VMEM((rows, 2 * width), bf16),
            pltpu.VMEM((rows, 128), f32),
            pltpu.VMEM((rows, chans), bf16),
            pltpu.VMEM((edge, chans), bf16),
            pltpu.VMEM((chans // 128, rows + edge, 128), f32),
            pltpu.VMEM((rows, chans), f32),
            pltpu.VMEM((rows, 256), f32),
            pltpu.VMEM((rows, 256), f32),
            pltpu.VMEM((seats, height, rank), bf16),
            pltpu.VMEM((pairs, 256, 2 * rows), bf16),
            pltpu.VMEM((keys_wide, heads * NOPE_DIM), bf16),
            pltpu.VMEM((keys_wide, 128), bf16),
            pltpu.VMEM((pairs, value_rows, keys_wide), bf16),
            pltpu.VMEM((max(pairs, 8), 2 * rows), f32),
            pltpu.VMEM((pairs, 2 * rows // 256, value_rows, 256), f32),
            pltpu.VMEM((2, keys_wide, 2 * rows), f32),
            pltpu.VMEM((heads * VALUE_DIM, rows), f32),
            pltpu.VMEM((2, rows, 128), f32),
            pltpu.VMEM((2, rows, 128), f32),
            pltpu.VMEM((pieces, rows, width // pieces), bf16),
            pltpu.VMEM((pieces, rows, width // pieces), bf16),
            dma((len(matrices),)),
        ]
        + [dma] * 11
        + [
            dma((pieces,)),
            dma((pieces,)),
            dma((max(layers - 1, 1),)),
            dma((layers, PLANE - 1)),
            dma((seats,)),
            dma((seats,)),
            dma((seats,)),
        ],
        compiler_params=pltpu.CompilerParams(
            vmem_limit_bytes=60 << 20, collective_id=0, has_side_effects=True
        ),
        name="layer",
    )(tokens, input_gain, kv_gain, base, seat, taps, ln_gain, ln_bias, att_gain, conv_gain, *matrices)


def gathered_kernel(q_ref, lat_ref, kup_ref, vup_ref, o_ref, kt, vt, run_max, acc):
    heads, rows, lanes = q_ref.shape
    blocks = lat_ref.shape[0]
    rank = kup_ref.shape[1]
    nope = kup_ref.shape[0] // heads
    vdim = vup_ref.shape[0] // heads
    rot = lat_ref.shape[1] - rank
    wide = kt.shape[2]
    group = wide // rows
    me = lax.axis_index("sp")
    last = me // group
    kt[:, nope + rot :, :] = jnp.zeros((heads, lanes - nope - rot, wide), jnp.bfloat16)
    vt[:, vdim:, :] = jnp.ones((heads, lanes - vdim, wide), jnp.bfloat16)

    def expand(block):
        for part in range(group):
            src = jnp.minimum(block * group + part, blocks - 1)
            lat = lat_ref[src, :rank, :]
            turned = lat_ref[src, rank:, :]
            cols = slice(part * rows, (part + 1) * rows)
            keys = jnp.dot(kup_ref[...], lat, preferred_element_type=jnp.float32)
            values = jnp.dot(vup_ref[...], lat, preferred_element_type=jnp.float32)
            for head in range(heads):
                kt[head, :nope, cols] = keys[head * nope : (head + 1) * nope].astype(jnp.bfloat16)
                kt[head, nope : nope + rot, cols] = turned
                vt[head, :vdim, cols] = values[head * vdim : (head + 1) * vdim].astype(
                    jnp.bfloat16
                )

    def weigh(head, scores, top):
        weights = jnp.exp2(scores - top).astype(jnp.bfloat16)
        return lax.dot_general(
            weights, vt[head], (((1,), (1,)), ((), ())), preferred_element_type=jnp.float32
        )

    expand(last)
    key_pos = last * wide + lax.broadcasted_iota(jnp.int32, (rows, wide), 1)
    query_pos = me * rows + lax.broadcasted_iota(jnp.int32, (rows, wide), 0)
    hidden = key_pos > query_pos
    for head in range(heads):
        scores = jnp.dot(q_ref[head], kt[head], preferred_element_type=jnp.float32)
        scores = jnp.where(hidden, far_below, scores)
        top = jnp.max(scores, axis=1, keepdims=True)
        run_max[head] = jnp.broadcast_to(top, (rows, lanes))
        acc[head] = weigh(head, scores, top)

    def visit(step, carry):
        expand(step)
        for head in range(heads):
            scores = jnp.dot(q_ref[head], kt[head], preferred_element_type=jnp.float32)
            old = run_max[head]
            top = jnp.maximum(old[:, :1], jnp.max(scores, axis=1, keepdims=True))
            wide_top = jnp.broadcast_to(top, (rows, lanes))
            run_max[head] = wide_top
            acc[head] = acc[head] * jnp.exp2(old - wide_top) + weigh(head, scores, top)
        return carry

    lax.fori_loop(0, last, visit, 0)
    lane = lax.broadcasted_iota(jnp.int32, (rows, lanes), 1)
    for pair in range(heads // 2):
        halves = []
        for head in (2 * pair, 2 * pair + 1):
            total = acc[head]
            halves.append(total / pltpu.roll(total, vdim, axis=1))
        both = jnp.where(lane < vdim, halves[0], pltpu.roll(halves[1], vdim, axis=1))
        o_ref[:, pair * lanes : (pair + 1) * lanes] = both.astype(jnp.bfloat16)


def gathered_attention(q_heads, lat_all, key_up_t, value_up_t):
    heads, rows, lanes = q_heads.shape
    blocks = lat_all.shape[0]
    wide = 2 * rows if blocks % 2 == 0 else rows
    vmem = pl.BlockSpec(memory_space=pltpu.VMEM)
    return pl.pallas_call(
        gathered_kernel,
        out_shape=jax.ShapeDtypeStruct((rows, value_up_t.shape[0]), jnp.bfloat16),
        in_specs=[vmem] * 4,
        out_specs=vmem,
        scratch_shapes=[
            pltpu.VMEM((heads, lanes, wide), jnp.bfloat16),
            pltpu.VMEM((heads, lanes, wide), jnp.bfloat16),
            pltpu.VMEM((heads, rows, lanes), jnp.float32),
            pltpu.VMEM((heads, rows, lanes), jnp.float32),
        ],
        compiler_params=pltpu.CompilerParams(vmem_limit_bytes=48 << 20),
        cost_estimate=pl.CostEstimate(
            flops=20_000_000_000, bytes_accessed=8 << 20, transcendentals=20_000_000
        ),
        name="gathered_attention",
    )(q_heads, lat_all, key_up_t, value_up_t)


def conv_kernel(gated_ref, rim_ref, taps_ref, out_ref, wide):
    rows, chans = gated_ref.shape
    rim = rim_ref.shape[0]
    taps = taps_ref.shape[0]
    chunk = 64
    for part in range(chans // 128):
        cols = slice(part * 128, (part + 1) * 128)
        wide[part, :rim, :] = rim_ref[:, cols].astype(jnp.float32)
        wide[part, rim:, :] = gated_ref[:, cols].astype(jnp.float32)
        coeff = taps_ref[:, cols]

        def band(step, carry):
            base = step * chunk
            total = jnp.zeros((chunk, 128), jnp.float32)
            for tap in range(taps):
                total = total + coeff[tap : tap + 1, :] * wide[
                    part, pl.ds(base + (rim - taps + 1 + tap), chunk), :
                ]
            out_ref[pl.ds(pl.multiple_of(base, chunk), chunk), cols] = total
            return carry

        lax.fori_loop(0, rows // chunk, band, 0)


def convolve(gated, rim, taps):
    rows, chans = gated.shape
    vmem = pl.BlockSpec(memory_space=pltpu.VMEM)
    return pl.pallas_call(
        conv_kernel,
        out_shape=jax.ShapeDtypeStruct((rows, chans), jnp.float32),
        in_specs=[vmem] * 3,
        out_specs=vmem,
        scratch_shapes=[pltpu.VMEM((chans // 128, rows + rim.shape[0], 128), jnp.float32)],
        cost_estimate=pl.CostEstimate(
            flops=2 * rows * chans * 31, bytes_accessed=2 << 20, transcendentals=0
        ),
        name="depthwise",
    )(gated, rim, taps)


def shards(
    tokens,
    input_gain,
    query_weight,
    query_rot_weight,
    kv_down,
    rot_down,
    kv_gain,
    key_up,
    value_up,
    conv_value_weight,
    conv_gate_weight,
    conv_taps,
    conv_ln_gain,
    conv_ln_bias,
    att_out_gain,
    conv_out_gain,
    att_out_weight,
    conv_out_weight,
):
    tok_rows = tokens.shape[0]
    heads_here = key_up.shape[1] // NOPE_DIM
    chan_here = conv_taps.shape[1]
    weight_list = (
        query_weight,
        query_rot_weight,
        kv_down,
        rot_down,
        conv_value_weight,
        conv_gate_weight,
    )
    seats = lax.axis_size("sp")
    if (
        lax.axis_size("tp") == 2
        and seats % PLANE == 0
        and tok_rows % 128 == 0
        and heads_here % 2 == 0
    ):
        gains = (
            input_gain, kv_gain, conv_ln_gain, conv_ln_bias, att_out_gain, conv_out_gain
        )
        return fused(
            tokens,
            tuple(gain[None, :] for gain in gains),
            (
                kv_down, rot_down.T, conv_gate_weight, conv_value_weight, query_weight,
                query_rot_weight, key_up, value_up, att_out_weight, conv_out_weight,
            ),
            conv_taps,
            seats,
        )
    whole_rows = lax.all_gather(tokens, "tp", axis=1, tiled=True).astype(jnp.float32)
    scaled = (whole_rows * input_gain[None, :]).astype(jnp.bfloat16)
    row_scale = lax.rsqrt(jnp.mean(whole_rows * whole_rows, axis=1, keepdims=True) + norm_eps)

    def add_product(weight):
        return jnp.dot(scaled, weight, preferred_element_type=jnp.float32)

    summed = tuple((add_product(weight) for weight in weight_list))
    q_acc, qrot_acc, latent_raw, rot_acc, value_acc, gate_acc = summed
    positions = lax.axis_index("sp") * tok_rows + jnp.arange(tok_rows, dtype=jnp.int32)
    cos_table, sine_table = rotary_tables(positions, ROT_DIM // 2)
    fold = math.log2(math.e) / math.sqrt(NOPE_DIM + ROT_DIM)
    query_scale = row_scale * fold
    plain_q = (q_acc * query_scale).reshape(tok_rows, heads_here, NOPE_DIM)
    turned_q = rotate_half(
        (qrot_acc * query_scale).reshape(tok_rows, heads_here, ROT_DIM),
        cos_table[:, None, :],
        sine_table[:, None, :],
    )
    blank = jnp.zeros((tok_rows, heads_here, 128 - NOPE_DIM - ROT_DIM), jnp.float32)
    q_heads = jnp.transpose(
        jnp.concatenate([plain_q, turned_q, blank], axis=2).astype(jnp.bfloat16), (1, 0, 2)
    )
    latent = (
        latent_raw
        * lax.rsqrt(jnp.mean(latent_raw * latent_raw, axis=1, keepdims=True) + norm_eps)
        * kv_gain[None, :]
    ).astype(jnp.bfloat16)
    key_rot = rotate_half(rot_acc * row_scale, cos_table, sine_table).astype(jnp.bfloat16)
    gated_input = (value_acc * row_scale * jax.nn.sigmoid(gate_acc * row_scale)).astype(
        jnp.bfloat16
    )
    packed = jnp.concatenate([latent.T, key_rot.T], axis=0)
    rim_rows = shifted(gated_input[tok_rows - (KERNEL + 1) :], "sp", 1)
    conv_out = convolve(gated_input, rim_rows, conv_taps)
    moment_one, moment_two = lax.psum(
        (jnp.sum(conv_out, axis=1), jnp.sum(conv_out * conv_out, axis=1)), "tp"
    )
    mean_val = moment_one / CONV_CH
    spread = moment_two / CONV_CH - mean_val * mean_val
    normed = (conv_out - mean_val[:, None]) * lax.rsqrt(spread + norm_eps)[:, None]
    swished = jax.nn.silu(normed * conv_ln_gain[None, :] + conv_ln_bias[None, :])
    lat_all = lax.all_gather(packed, "sp", axis=0)
    attended = gathered_attention(q_heads, lat_all, key_up.T, value_up.T).astype(jnp.float32)
    att_sq, conv_sq = lax.psum(
        (
            jnp.sum(attended * attended, axis=1, keepdims=True),
            jnp.sum(swished * swished, axis=1, keepdims=True),
        ),
        "tp",
    )
    att_mixed = (
        attended * lax.rsqrt(att_sq / ATT_WIDTH + norm_eps) * att_out_gain[None, :]
    ).astype(jnp.bfloat16)
    conv_mixed = (
        swished * lax.rsqrt(conv_sq / CONV_CH + norm_eps) * conv_out_gain[None, :]
    ).astype(jnp.bfloat16)
    share = (
        jnp.dot(att_mixed, att_out_weight, preferred_element_type=jnp.float32)
        + jnp.dot(conv_mixed, conv_out_weight, preferred_element_type=jnp.float32)
    ).astype(jnp.bfloat16)
    return lax.psum_scatter(share, "tp", scatter_dimension=1, tiled=True)


def solution(mesh):
    return jax.shard_map(
        shards,
        mesh=mesh,
        in_specs=(
            P("sp", "tp"),
            P(),
            P(None, "tp"),
            P(None, "tp"),
            P(),
            P(),
            P(),
            P(None, "tp"),
            P(None, "tp"),
            P(None, "tp"),
            P(None, "tp"),
            P(None, "tp"),
            P("tp"),
            P("tp"),
            P("tp"),
            P("tp"),
            P("tp", None),
            P("tp", None),
        ),
        out_specs=P("sp", "tp"),
        check_vma=False,
    )
```

time: 76.6 us -> 55.8 us (0.73)
  Pallas kernels: 68.4 us -> 53.5 us
  local copies, waits for them, and re-layouts: 7.03 us -> 2.06 us
  other arithmetic: 0.8 us -> 0 us
    pallas_call x3 -> x1, Pallas kernels: 68.4 us -> 53.5 us  [fused(): pl.pallas_call(layer_kernel, out_shape=jax.ShapeDtypeStruct((rows, width)...]
    unnamed x9 -> x1, local copies, waits for them, and re-layouts: 7.03 us -> 2.06 us
    sin x1 -> x0, other arithmetic: 0.79 us -> none  [rotary_tables(): return (jnp.cos(angles), jnp.sin(angles))]
where the time goes in v1:
time: 55.8 us; the launch traced here: 55.5 us
  Pallas kernels  53.5 us (96%)
  local copies, waits for them, and re-layouts  2.06 us (4%)
    pallas_call x1, Pallas kernels, fused(): pl.pallas_call(layer_kernel, out_shape=jax.ShapeDtypeStruct((rows, width)...  53.5 us
    unnamed x1, local copies, waits for them, and re-layouts  2.06 us

profile of v1, /device:TPU:25, one launch (start us, length us, event | category | flops | bytes accessed | tf_op | source)
XLA Modules:
  0.0 55.5 jit_solution(4926120809755939316)
XLA Ops:
  0.0 53.5 %layer.1 = bf16[384,1024]{1,0:T(8,128)(2,1)} custom-call(bf16[384,1024]{1,0:T(8,128)(2,1)} %tok_hbm.1, f32[1,2048]{1,0:T(1,128)} %bitcast.8, f32[1,256]{1,0:T(1,128)} %bitcast.13, f32[32,384]{1,0:T(8,128)} %constant.4.clone.base_ref, f32[32,128]{1,0:T(8,128)} %constant.5.clone.seat_ref, f32[31,512]{1,0:T(8,128)} %taps_ref.1, f32[1,512]{1,0:T(1,128)} %bitcast.9, ...), custom_call_target="tpu_custom_call" | custom-call | tf_op jit(solution)/shard_map/layer/pallas_call | solution.py:567
  53.5 2.1 %copy.22 = bf16[384,1024]{1,0:T(8,128)(2,1)} copy(bf16[384,1024]{1,0:T(8,128)(2,1)} %layer.1) | data formatting | bytes 1572864

commit v2 on v1

--- a/solution.py
+++ b/solution.py
@@ -75,9 +75,10 @@
     out_ref,
     kvd, rotw, cgw, cvw, qw, qrw, kup, vup, att_w, conv_w, vup_t,
     tok, landed, scaled, narrow, gated, rim, wide, conv, sq_mine, sq_other,
-    lat_ref, q2, kn, kr, vt, run_max, acc, s_ref, att_t, end_mine, end_other, part, arrived,
-    w_sem, tok_load, tok_send, tok_recv, rim_send, rim_recv, sq_send, sq_recv,
-    csq_send, csq_recv, asq_send, asq_recv, part_send, part_recv,
+    lat_ref, q2, kn, kr, vt, run_max, acc, s_ref, att_t, end_mine, end_other,
+    att_sq, att_sq_other, att_act, conv_act,
+    w_sem, w_send, w_recv, tok_load, tok_send, tok_recv, rim_send, rim_recv, sq_send, sq_recv,
+    csq_send, csq_recv, asq_send, asq_recv, conv_send, conv_recv, att_send, att_recv,
     col_send, plane_send, core_send, link_recv, core_recv,
 ):
     mine = lax.axis_index("tp")
@@ -95,20 +96,28 @@
     ahead = {"sp": (me + 1) % seats, "tp": mine}
     behind = {"sp": (me + seats - 1) % seats, "tp": mine}
 
+    def columns(owner):
+        return pl.ds(pl.multiple_of(owner * width, 128), width)
+
     loads = [
         pltpu.make_async_copy(src, dst, w_sem.at[index])
         for index, (src, dst) in enumerate(
             (
                 (kvd_hbm, kvd), (rotw_hbm, rotw), (cgw_hbm, cgw), (cvw_hbm, cvw),
                 (qw_hbm, qw), (qrw_hbm, qrw), (kup_hbm, kup), (vup_hbm, vup),
-                (att_hbm, att_w), (conv_hbm, conv_w),
+                (att_hbm.at[:, columns(mine)], att_w.at[0]),
+                (conv_hbm.at[:, columns(mine)], conv_w.at[0]),
             )
         )
     ]
     fetch = pltpu.make_async_copy(tok_hbm, tok, tok_load)
     fetch.start()
-    for load in loads:
+    for load in loads[:2]:
         load.start()
+    gifts = [
+        push(src.at[:, columns(1 - mine)], dst.at[1], w_send.at[index], w_recv.at[index], other)
+        for index, (src, dst) in enumerate(((att_hbm, att_w), (conv_hbm, conv_w)))
+    ]
 
     def spot_at(distance):
         return (spot + distance) % PLANE
@@ -117,21 +126,18 @@
         return {"sp": layer_id * PLANE + spot_id, "tp": mine}
 
     barrier = pltpu.get_barrier_semaphore()
-    peers = (
-        [at((layer + d) % layers, spot) for d in range(1, layers)]
-        + [at(layer, spot_at(d)) for d in range(1, PLANE)]
-        + [other]
-    )
+    peers = [at(layer, spot_at(d)) for d in range(1, PLANE)] + [other]
     for peer in peers:
         pl.semaphore_signal(barrier, inc=1, device_id=peer, device_id_type=MESH)
-
-    @pl.when(me < seats - 1)
-    def _():
-        pl.semaphore_signal(barrier, inc=1, device_id=ahead, device_id_type=MESH)
-
-    @pl.when(me > 0)
-    def _():
-        pl.semaphore_signal(barrier, inc=1, device_id=behind, device_id_type=MESH)
+    above = at(jnp.minimum(layer + 1, layers - 1), spot)
+    below = at(jnp.maximum(layer - 1, 0), spot)
+    for condition, peer in (
+        (layer < layers - 1, above), (layer > 0, below), (me < seats - 1, ahead), (me > 0, behind),
+    ):
+
+        @pl.when(condition)
+        def _(peer=peer):
+            pl.semaphore_signal(barrier, inc=1, device_id=peer, device_id_type=MESH)
 
     q2[...] = jnp.zeros(q2.shape, jnp.bfloat16)
     pairs, _, both = q2.shape
@@ -140,11 +146,18 @@
     ones_high = vt.shape[1] - VALUE_DIM
     vt[:, ones_low:ones_high, :] = jnp.ones((pairs, ones_high - ones_low, keys_wide), jnp.bfloat16)
     pl.semaphore_wait(
-        barrier, len(peers) + jnp.minimum(me, 1) + jnp.minimum(seats - 1 - me, 1)
+        barrier,
+        len(peers)
+        + jnp.minimum(me, 1)
+        + jnp.minimum(seats - 1 - me, 1)
+        + jnp.minimum(layer, 1)
+        + jnp.minimum(layers - 1 - layer, 1),
     )
     fetch.wait()
     tok_copy = push(tok, landed, tok_send, tok_recv, other)
     tok_copy.start()
+    for load in loads[2:]:
+        load.start()
 
     def place(block, index):
         cols = pl.ds(pl.multiple_of(index * width, 128), width)
@@ -153,8 +166,6 @@
         return jnp.sum(full * full, axis=1, keepdims=True)
 
     squares = place(tok, mine)
-    loads[7].wait()
-    vup_t[...] = vup[...].astype(jnp.float32).T.astype(jnp.bfloat16)
     column = lax.broadcasted_iota(jnp.int32, seat_ref.shape, 1)
     seat_turn = jnp.sum(
         jnp.where(column == me, seat_ref[...], 0.0), axis=1, keepdims=True
@@ -203,14 +214,14 @@
             else jnp.zeros((ROT_DIM, 128), jnp.bfloat16)
         )
 
-    def column_copy(distance):
-        return push(
-            lat_ref.at[me, half],
-            lat_ref.at[me, half],
-            col_send.at[distance - 1],
-            link_recv.at[me],
-            at(jnp.minimum(layer + distance, layers - 1), spot),
-        )
+    def column_copy(block):
+        spread = lat_ref.at[block, half]
+        return push(spread, spread, col_send.at[block // PLANE], link_recv.at[block], above)
+
+    def rise(block):
+        @pl.when(layer + 1 < layers)
+        def _():
+            column_copy(block).start()
 
     def plane_copy(block, distance):
         return push(
@@ -225,13 +236,11 @@
         spread = lat_ref.at[block, half]
         return push(spread, spread, core_send.at[block], core_recv.at[block], other)
 
+    rise(me)
     for d in range(1, PLANE):
         plane_copy(me, d).start()
-    for d in range(1, layers):
-
-        @pl.when(layer + d < layers)
-        def _(d=d):
-            column_copy(d).start()
+    for gift in gifts:
+        gift.start()
 
     def arrive(block):
         spread = lat_ref.at[block, half]
@@ -242,6 +251,7 @@
         def _():
             block = (layer - step) * PLANE + spot
             arrive(block)
+            rise(block)
             for d in range(1, PLANE):
                 plane_copy(block, d).start()
             core_copy(block).start()
@@ -280,7 +290,8 @@
             turned[head * ROT_DIM : (head + 1) * ROT_DIM]
         ).astype(jnp.bfloat16)
 
-    relay(1)
+    loads[7].wait()
+    vup_t[...] = vup[...].astype(jnp.float32).T.astype(jnp.bfloat16)
 
     @pl.when(me > 0)
     def _():
@@ -309,6 +320,8 @@
             return carry
 
         lax.fori_loop(0, rows // chunk, band_step, 0)
+        if slab == 1:
+            relay(1)
 
     values = conv[...]
     for slot, total in enumerate((values, values * values)):
@@ -318,19 +331,24 @@
     sums = push(sq_mine, sq_other, sq_send, sq_recv, other)
     sums.start()
     hand_over(0)
-    sums.wait()
-    moments = (sq_mine[...] + sq_other[...]) / CONV_CH
-    mean_val = moments[:, :1]
-    spread_val = moments[:, 128:129] - mean_val * mean_val
-    normed = (values - mean_val) * lax.rsqrt(spread_val + norm_eps)
-    swished = jax.nn.silu(normed * ln_gain_ref[...] + ln_bias_ref[...])
-    conv[...] = swished
-    end_mine[0] = jnp.broadcast_to(
-        jnp.sum(swished * swished, axis=1, keepdims=True), (rows, 128)
-    )
-    conv_sum = push(end_mine.at[0], end_other.at[0], csq_send, csq_recv, other)
-    conv_sum.start()
-    relay(2)
+
+    def activate():
+        sums.wait()
+        values = conv[...]
+        moments = (sq_mine[...] + sq_other[...]) / CONV_CH
+        mean_val = moments[:, :1]
+        spread_val = moments[:, 128:129] - mean_val * mean_val
+        normed = (values - mean_val) * lax.rsqrt(spread_val + norm_eps)
+        swished = jax.nn.silu(normed * ln_gain_ref[...] + ln_bias_ref[...])
+        conv_act[0] = (swished * conv_gain_ref[...]).astype(jnp.bfloat16)
+        end_mine[...] = jnp.broadcast_to(
+            jnp.sum(swished * swished, axis=1, keepdims=True), (rows, 128)
+        )
+        conv_sum.start()
+        conv_copy.start()
+
+    conv_sum = push(end_mine, end_other, csq_send, csq_recv, other)
+    conv_copy = push(conv_act.at[0], conv_act.at[1], conv_send, conv_recv, other)
 
     def gathered(step):
         for d in range(1, PLANE):
@@ -389,8 +407,7 @@
 
         tops = [score(0, index) for index in range(strips)]
         for pair in range(pairs):
-            if pair == pairs // 2:
-                middle()
+            middle(pair)
             top = tops[0]
             for value in tops[1:]:
                 top = jnp.maximum(top, value)
@@ -432,8 +449,12 @@
     gathered(0)
     expand(layer)
 
-    def first_middle():
-        hand_over(1)
+    def first_middle(pair):
+        if pair == 1:
+            relay(2)
+            activate()
+        if pair == pairs - 1:
+            hand_over(1)
 
     attend(True, hidden, first_middle)
 
@@ -442,9 +463,11 @@
             core_copy((layer - step) * PLANE + spot_at(d)).wait_recv()
         expand(layer - step)
 
-        def middle():
-            hand_over(step + 1)
-            relay(step + 2)
+        def middle(pair):
+            if pair == 1:
+                relay(step + 2)
+            if pair == pairs - 1:
+                hand_over(step + 1)
 
         attend(False, None, middle)
         return carry
@@ -465,63 +488,54 @@
                     total[base : base + VALUE_DIM] / total[ones_low - low : ones_low - low + 1]
                 )
             low = (2 * pair + side) * VALUE_DIM
-            att_t[low : low + VALUE_DIM, :] = jnp.concatenate(pieces, axis=1)
-    attended = att_t[...].T.astype(jnp.bfloat16).astype(jnp.float32)
-    end_mine[1] = jnp.broadcast_to(
-        jnp.sum(attended * attended, axis=1, keepdims=True), (rows, 128)
-    )
-    att_sum = push(end_mine.at[1], end_other.at[1], asq_send, asq_recv, other)
+            att_t[low : low + VALUE_DIM, :] = (
+                jnp.concatenate(pieces, axis=1).astype(jnp.bfloat16).astype(jnp.float32)
+            )
+    attended = att_t[...]
+    att_sq[...] = jnp.broadcast_to(
+        jnp.sum(attended * attended, axis=0, keepdims=True), att_sq.shape
+    )
+    att_act[0] = (attended.T * att_gain_ref[...]).astype(jnp.bfloat16)
+    att_sum = push(att_sq, att_sq_other, asq_send, asq_recv, other)
     att_sum.start()
+    att_copy = push(att_act.at[0], att_act.at[1], att_send, att_recv, other)
+    att_copy.start()
+    for index in (8, 9):
+        loads[index].wait()
+    for gift in gifts:
+        gift.wait()
     conv_sum.wait()
-    conv_scale = lax.rsqrt((end_mine[0] + end_other[0])[:, :1] / CONV_CH + norm_eps)
-    conv_mixed = (conv[...] * conv_scale * conv_gain_ref[...]).astype(jnp.bfloat16)
-    att_mixed = (attended * att_gain_ref[...]).astype(jnp.bfloat16)
-    loads[8].wait()
-    loads[9].wait()
-    pieces = part.shape[0]
-    piece = part.shape[2]
-
-    def products(owner, index):
-        cols = pl.ds(pl.multiple_of(owner * width + index * piece, 128), piece)
-        return (
-            jnp.dot(att_mixed, att_w[:, cols], preferred_element_type=jnp.float32),
-            jnp.dot(conv_mixed, conv_w[:, cols], preferred_element_type=jnp.float32),
-        )
-
-    waiting = [products(1 - mine, index) for index in range(pieces)]
+    conv_copy.wait()
+    conv_scale = lax.rsqrt((end_mine[...] + end_other[...])[:, :1] / CONV_CH + norm_eps)
+
+    def product(activations, weight):
+        return jnp.dot(activations, weight, preferred_element_type=jnp.float32)
+
+    base_part = (
+        product(conv_act[0], conv_w[0]) + product(conv_act[1], conv_w[1])
+    ) * conv_scale
+    own_part = product(att_act[0], att_w[0])
     att_sum.wait()
-    att_scale = lax.rsqrt((end_mine[1] + end_other[1])[:, :1] / ATT_WIDTH + norm_eps)
-    copies = []
-    for index, (from_att, from_conv) in enumerate(waiting):
-        part[index] = (from_att * att_scale + from_conv).astype(jnp.bfloat16)
-        copy = push(
-            part.at[index], arrived.at[index], part_send.at[index], part_recv.at[index], other
-        )
-        copy.start()
-        copies.append(copy)
-    for index in range(pieces):
-        from_att, from_conv = products(mine, index)
-        own = (from_att * att_scale + from_conv).astype(jnp.bfloat16).astype(jnp.float32)
-        copies[index].wait()
-        out_ref[:, index * piece : (index + 1) * piece] = (
-            own + arrived[index].astype(jnp.float32)
-        ).astype(jnp.bfloat16)
+    squares_t = jnp.broadcast_to(att_sq[:1] + att_sq_other[:1], (128, rows)).T
+    att_scale = lax.rsqrt(squares_t[:, :1] / ATT_WIDTH + norm_eps)
+    att_copy.wait()
+    out_ref[...] = (
+        (own_part + product(att_act[1], att_w[1])) * att_scale + base_part
+    ).astype(jnp.bfloat16)
 
     @pl.when(me < seats - 1)
     def _():
         rim_copy.wait_send()
-
-    for d in range(1, layers):
-
-        @pl.when(layer + d < layers)
-        def _(d=d):
-            column_copy(d).wait_send()
 
     def settle(step, carry):
         base = (layer - step) * PLANE
         for d in range(1, PLANE):
             plane_copy(base + spot, d).wait_send()
             core_copy(base + spot_at(d)).wait_send()
+
+        @pl.when(layer + 1 < layers)
+        def _():
+            column_copy(base + spot).wait_send()
 
         @pl.when(step > 0)
         def _():
@@ -558,7 +572,6 @@
     anywhere = pl.BlockSpec(memory_space=pltpu.HBM)
     dma = pltpu.SemaphoreType.DMA
     edge = 32
-    pieces = 4
     bf16 = jnp.bfloat16
     f32 = jnp.float32
     value_rows = 2 * VALUE_DIM + 16
@@ -569,7 +582,10 @@
         out_shape=jax.ShapeDtypeStruct((rows, width), bf16),
         in_specs=[anywhere] + [vmem] * 9 + [anywhere] * 10,
         out_specs=vmem,
-        scratch_shapes=[pltpu.VMEM(matrix.shape, bf16) for matrix in matrices]
+        scratch_shapes=[pltpu.VMEM(matrix.shape, bf16) for matrix in matrices[:8]]
+        + [
+            pltpu.VMEM((2, matrix.shape[0], width), bf16) for matrix in matrices[8:]
+        ]
         + [
             pltpu.VMEM(matrices[7].shape[::-1], bf16),
             pltpu.VMEM((rows, width), bf16),
@@ -591,17 +607,19 @@
             pltpu.VMEM((pairs, 2 * rows // 256, value_rows, 256), f32),
             pltpu.VMEM((2, keys_wide, 2 * rows), f32),
             pltpu.VMEM((heads * VALUE_DIM, rows), f32),
-            pltpu.VMEM((2, rows, 128), f32),
-            pltpu.VMEM((2, rows, 128), f32),
-            pltpu.VMEM((pieces, rows, width // pieces), bf16),
-            pltpu.VMEM((pieces, rows, width // pieces), bf16),
+            pltpu.VMEM((rows, 128), f32),
+            pltpu.VMEM((rows, 128), f32),
+            pltpu.VMEM((8, rows), f32),
+            pltpu.VMEM((8, rows), f32),
+            pltpu.VMEM((2, rows, heads * VALUE_DIM), bf16),
+            pltpu.VMEM((2, rows, chans), bf16),
             dma((len(matrices),)),
+            dma((2,)),
+            dma((2,)),
         ]
-        + [dma] * 11
+        + [dma] * 15
         + [
-            dma((pieces,)),
-            dma((pieces,)),
-            dma((max(layers - 1, 1),)),
+            dma((layers,)),
             dma((layers, PLANE - 1)),
             dma((seats,)),
             dma((seats,)),

time: 55.8 us -> 50.9 us (0.912)
  the two profiles are of different devices: /device:TPU:25 before, /device:TPU:29 now
where the time goes in v2:
time: 50.9 us; the launch traced here: 50.7 us
  Pallas kernels  48.7 us (96%)
  local copies, waits for them, and re-layouts  2.06 us (4%)
    pallas_call x1, Pallas kernels, fused(): pl.pallas_call(layer_kernel, out_shape=jax.ShapeDtypeStruct((rows, width)...  48.7 us
    unnamed x1, local copies, waits for them, and re-layouts  2.06 us

profile of v2, /device:TPU:29, one launch (start us, length us, event | category | flops | bytes accessed | tf_op | source)
XLA Modules:
  0.0 50.7 jit_solution(5070941199877579778)
XLA Ops:
  0.0 48.7 %layer.1 = bf16[384,1024]{1,0:T(8,128)(2,1)} custom-call(bf16[384,1024]{1,0:T(8,128)(2,1)} %tok_hbm.1, f32[1,2048]{1,0:T(1,128)} %bitcast.8, f32[1,256]{1,0:T(1,128)} %bitcast.13, f32[32,384]{1,0:T(8,128)} %constant.4.clone.base_ref, f32[32,128]{1,0:T(8,128)} %constant.5.clone.seat_ref, f32[31,512]{1,0:T(8,128)} %taps_ref.1, f32[1,512]{1,0:T(1,128)} %bitcast.9, ...), custom_call_target="tpu_custom_call" | custom-call | tf_op jit(solution)/shard_map/layer/pallas_call | solution.py:580
  48.7 2.1 %copy.22 = bf16[384,1024]{1,0:T(8,128)(2,1)} copy(bf16[384,1024]{1,0:T(8,128)(2,1)} %layer.1) | data formatting | bytes 1572864

commit v3 on v2

--- a/solution.py
+++ b/solution.py
@@ -1,3 +1,4 @@
+import functools
 import math
 
 import jax
@@ -76,10 +77,10 @@
     kvd, rotw, cgw, cvw, qw, qrw, kup, vup, att_w, conv_w, vup_t,
     tok, landed, scaled, narrow, gated, rim, wide, conv, sq_mine, sq_other,
     lat_ref, q2, kn, kr, vt, run_max, acc, s_ref, att_t, end_mine, end_other,
-    att_sq, att_sq_other, att_act, conv_act,
+    att_sq, att_sq_other, att_act, conv_act, out_stage,
     w_sem, w_send, w_recv, tok_load, tok_send, tok_recv, rim_send, rim_recv, sq_send, sq_recv,
     csq_send, csq_recv, asq_send, asq_recv, conv_send, conv_recv, att_send, att_recv,
-    col_send, plane_send, core_send, link_recv, core_recv,
+    col_send, plane_send, core_send, link_recv, core_recv, out_sem,
 ):
     mine = lax.axis_index("tp")
     me = lax.axis_index("sp")
@@ -141,10 +142,12 @@
 
     q2[...] = jnp.zeros(q2.shape, jnp.bfloat16)
     pairs, _, both = q2.shape
-    keys_wide = kn.shape[0]
+    keys_wide = kn.shape[1]
     ones_low = VALUE_DIM
-    ones_high = vt.shape[1] - VALUE_DIM
-    vt[:, ones_low:ones_high, :] = jnp.ones((pairs, ones_high - ones_low, keys_wide), jnp.bfloat16)
+    ones_high = vt.shape[2] - VALUE_DIM
+    vt[:, :, ones_low:ones_high, :] = jnp.ones(
+        (2, pairs, ones_high - ones_low, keys_wide), jnp.bfloat16
+    )
     pl.semaphore_wait(
         barrier,
         len(peers)
@@ -293,6 +296,29 @@
     loads[7].wait()
     vup_t[...] = vup[...].astype(jnp.float32).T.astype(jnp.bfloat16)
 
+    taps = taps_ref.shape[0]
+    chunk = 64
+
+    def band_step(step, carry, slab):
+        cols = slice(slab * 128, (slab + 1) * 128)
+        coeff = taps_ref[:, cols]
+        base = step * chunk
+        total = jnp.zeros((chunk, 128), jnp.float32)
+        for tap in range(taps):
+            total = total + coeff[tap : tap + 1, :] * wide[
+                slab, pl.ds(base + (edge - taps + 1 + tap), chunk), :
+            ]
+        conv[pl.ds(pl.multiple_of(base, chunk), chunk), cols] = total
+        return carry
+
+    slabs = conv.shape[1] // 128
+    for slab in range(slabs):
+        wide[slab, edge:, :] = gated[:, slab * 128 : (slab + 1) * 128].astype(jnp.float32)
+        lax.fori_loop(1, rows // chunk, functools.partial(band_step, slab=slab), 0)
+        if slab == slabs // 2:
+            relay(1)
+    hand_over(0)
+
     @pl.when(me > 0)
     def _():
         rim_copy.wait_recv()
@@ -301,27 +327,9 @@
     def _():
         rim[...] = jnp.zeros(rim.shape, jnp.bfloat16)
 
-    taps = taps_ref.shape[0]
-    chunk = 64
-    for slab in range(conv.shape[1] // 128):
-        cols = slice(slab * 128, (slab + 1) * 128)
-        wide[slab, :edge, :] = rim[:, cols].astype(jnp.float32)
-        wide[slab, edge:, :] = gated[:, cols].astype(jnp.float32)
-        coeff = taps_ref[:, cols]
-
-        def band_step(step, carry, slab=slab, cols=cols, coeff=coeff):
-            base = step * chunk
-            total = jnp.zeros((chunk, 128), jnp.float32)
-            for tap in range(taps):
-                total = total + coeff[tap : tap + 1, :] * wide[
-                    slab, pl.ds(base + (edge - taps + 1 + tap), chunk), :
-                ]
-            conv[pl.ds(pl.multiple_of(base, chunk), chunk), cols] = total
-            return carry
-
-        lax.fori_loop(0, rows // chunk, band_step, 0)
-        if slab == 1:
-            relay(1)
+    for slab in range(slabs):
+        wide[slab, :edge, :] = rim[:, slab * 128 : (slab + 1) * 128].astype(jnp.float32)
+        band_step(0, 0, slab)
 
     values = conv[...]
     for slot, total in enumerate((values, values * values)):
@@ -330,7 +338,6 @@
         )
     sums = push(sq_mine, sq_other, sq_send, sq_recv, other)
     sums.start()
-    hand_over(0)
 
     def activate():
         sums.wait()
@@ -354,51 +361,55 @@
         for d in range(1, PLANE):
             core_copy((layer - step) * PLANE + spot_at(d)).wait_recv()
 
-    span = 2 * rows
-
-    def expand(group):
-        for index in range(PLANE // 2):
-            blk = group * PLANE + 2 * index
-            cols = slice(index * span, (index + 1) * span)
-            lat = jnp.concatenate([lat_ref[blk, :rows, :], lat_ref[blk + 1, :rows, :]], axis=0)
-            kn[cols, :] = jnp.dot(
-                lat, kup[...], preferred_element_type=jnp.float32
-            ).astype(jnp.bfloat16)
-            values = lax.dot_general(
-                vup_t[...], lat, (((1,), (1,)), ((), ())), preferred_element_type=jnp.float32
-            ).astype(jnp.bfloat16)
-            for pair in range(pairs):
-                low = 2 * VALUE_DIM * pair
-                vt[pair, :ones_low, cols] = values[low : low + VALUE_DIM]
-                vt[pair, ones_high:, cols] = values[low + VALUE_DIM : low + 2 * VALUE_DIM]
-            for part_id in range(2):
-                pieces = []
-                for piece in range(rows // 128):
-                    band = rows + piece // across * ROT_DIM
-                    lanes = slice(piece % across * 128, piece % across * 128 + 128)
-                    pieces.append(lat_ref[blk + part_id, band : band + ROT_DIM, lanes])
-                rot = jnp.concatenate(pieces, axis=1).astype(jnp.float32)
-                rot = jnp.concatenate(
-                    [rot, jnp.zeros((128 - ROT_DIM, rows), jnp.float32)], axis=0
-                )
-                low = index * span + part_id * rows
-                kr[low : low + rows, :] = rot.T.astype(jnp.bfloat16)
-
     strip = 256
     strips = keys_wide // strip
+
+    def expand(group, slot, index):
+        pieces = []
+        low, left = index * strip, strip
+        while left > 0:
+            take = min(rows - low % rows, left)
+            pieces.append(
+                lat_ref[group * PLANE + low // rows, low % rows : low % rows + take, :]
+            )
+            low, left = low + take, left - take
+        lat = pieces[0] if len(pieces) == 1 else jnp.concatenate(pieces, axis=0)
+        cut = slice(index * strip, (index + 1) * strip)
+        kn[slot, cut, :] = jnp.dot(
+            lat, kup[...], preferred_element_type=jnp.float32
+        ).astype(jnp.bfloat16)
+        values = lax.dot_general(
+            vup_t[...], lat, (((1,), (1,)), ((), ())), preferred_element_type=jnp.float32
+        ).astype(jnp.bfloat16)
+        for pair in range(pairs):
+            low = 2 * VALUE_DIM * pair
+            vt[slot, pair, :ones_low, cut] = values[low : low + VALUE_DIM]
+            vt[slot, pair, ones_high:, cut] = values[low + VALUE_DIM : low + 2 * VALUE_DIM]
+        for blk in range(index, PLANE, strips):
+            pieces = []
+            for piece in range(rows // 128):
+                band = rows + piece // across * ROT_DIM
+                lanes = slice(piece % across * 128, piece % across * 128 + 128)
+                pieces.append(lat_ref[group * PLANE + blk, band : band + ROT_DIM, lanes])
+            rot = jnp.concatenate(pieces, axis=1).astype(jnp.float32)
+            rot = jnp.concatenate([rot, jnp.zeros((128 - ROT_DIM, rows), jnp.float32)], axis=0)
+            kr[slot, blk * rows : (blk + 1) * rows, :] = rot.T.astype(jnp.bfloat16)
+
     tiles = both // 256
     tile_rows = tuple(
         (
             0 if 256 * tile < rows else ones_low,
-            ones_high if 256 * (tile + 1) <= rows else vt.shape[1],
+            ones_high if 256 * (tile + 1) <= rows else vt.shape[2],
         )
         for tile in range(tiles)
     )
 
-    def attend(first, hidden, middle):
+    def attend(slot, first, hidden, middle, following):
         def score(pair, index):
             cut = slice(index * strip, (index + 1) * strip)
-            keys = jnp.concatenate([kn[cut, 128 * pair : 128 * pair + 128], kr[cut, :]], axis=1)
+            keys = jnp.concatenate(
+                [kn[slot, cut, 128 * pair : 128 * pair + 128], kr[slot, cut, :]], axis=1
+            )
             scores = jnp.dot(keys, q2[pair], preferred_element_type=jnp.float32)
             if hidden is not None:
                 scores = jnp.where(hidden(index), far_below, scores)
@@ -425,11 +436,13 @@
                 weights = jnp.exp2(s_ref[pair % 2, cut, :] - top).astype(jnp.bfloat16)
                 for tile, (low, high) in enumerate(tile_rows):
                     new = jnp.dot(
-                        vt[pair, low:high, cut],
+                        vt[slot, pair, low:high, cut],
                         weights[:, 256 * tile : 256 * (tile + 1)],
                         preferred_element_type=jnp.float32,
                     )
                     sums[tile] = new if sums[tile] is None else sums[tile] + new
+                if pair + 1 == pairs:
+                    expand(following, 1 - slot, index)
             for tile, (low, high) in enumerate(tile_rows):
                 new = sums[tile]
                 if not first:
@@ -447,29 +460,34 @@
 
     loads[6].wait()
     gathered(0)
-    expand(layer)
+    for index in range(strips):
+        expand(layer, 0, index)
+
+    def ready(step):
+        @pl.when(step <= layer)
+        def _():
+            for d in range(PLANE):
+                core_copy((layer - step) * PLANE + spot_at(d)).wait_recv()
 
     def first_middle(pair):
-        if pair == 1:
+        if pair == pairs // 2:
             relay(2)
+            hand_over(1)
             activate()
         if pair == pairs - 1:
-            hand_over(1)
-
-    attend(True, hidden, first_middle)
+            ready(1)
+
+    attend(0, True, hidden, first_middle, jnp.maximum(layer - 1, 0))
 
     def far(step, carry):
-        for d in range(PLANE):
-            core_copy((layer - step) * PLANE + spot_at(d)).wait_recv()
-        expand(layer - step)
-
         def middle(pair):
-            if pair == 1:
+            if pair == pairs // 2:
                 relay(step + 2)
+                hand_over(step + 1)
             if pair == pairs - 1:
-                hand_over(step + 1)
-
-        attend(False, None, middle)
+                ready(step + 1)
+
+        attend(step % 2, False, None, middle, jnp.maximum(layer - step - 1, 0))
         return carry
 
     lax.fori_loop(1, layer + 1, far, 0)
@@ -519,9 +537,18 @@
     squares_t = jnp.broadcast_to(att_sq[:1] + att_sq_other[:1], (128, rows)).T
     att_scale = lax.rsqrt(squares_t[:, :1] / ATT_WIDTH + norm_eps)
     att_copy.wait()
-    out_ref[...] = (
-        (own_part + product(att_act[1], att_w[1])) * att_scale + base_part
-    ).astype(jnp.bfloat16)
+    leaves = []
+    for index in range(width // 256):
+        cols = slice(index * 256, (index + 1) * 256)
+        out_stage[:, cols] = (
+            (own_part[:, cols] + product(att_act[1], att_w[1, :, cols])) * att_scale
+            + base_part[:, cols]
+        ).astype(jnp.bfloat16)
+        leave = pltpu.make_async_copy(
+            out_stage.at[:, cols], out_ref.at[:, cols], out_sem.at[index]
+        )
+        leave.start()
+        leaves.append(leave)
 
     @pl.when(me < seats - 1)
     def _():
@@ -544,6 +571,8 @@
         return carry
 
     lax.fori_loop(0, layer + 1, settle, 0)
+    for leave in leaves:
+        leave.wait()
 
 
 def angle_tables(seats, rows):
@@ -581,7 +610,7 @@
         layer_kernel,
         out_shape=jax.ShapeDtypeStruct((rows, width), bf16),
         in_specs=[anywhere] + [vmem] * 9 + [anywhere] * 10,
-        out_specs=vmem,
+        out_specs=anywhere,
         scratch_shapes=[pltpu.VMEM(matrix.shape, bf16) for matrix in matrices[:8]]
         + [
             pltpu.VMEM((2, matrix.shape[0], width), bf16) for matrix in matrices[8:]
@@ -600,9 +629,9 @@
             pltpu.VMEM((rows, 256), f32),
             pltpu.VMEM((seats, height, rank), bf16),
             pltpu.VMEM((pairs, 256, 2 * rows), bf16),
-            pltpu.VMEM((keys_wide, heads * NOPE_DIM), bf16),
-            pltpu.VMEM((keys_wide, 128), bf16),
-            pltpu.VMEM((pairs, value_rows, keys_wide), bf16),
+            pltpu.VMEM((2, keys_wide, heads * NOPE_DIM), bf16),
+            pltpu.VMEM((2, keys_wide, 128), bf16),
+            pltpu.VMEM((2, pairs, value_rows, keys_wide), bf16),
             pltpu.VMEM((max(pairs, 8), 2 * rows), f32),
             pltpu.VMEM((pairs, 2 * rows // 256, value_rows, 256), f32),
             pltpu.VMEM((2, keys_wide, 2 * rows), f32),
@@ -613,6 +642,7 @@
             pltpu.VMEM((8, rows), f32),
             pltpu.VMEM((2, rows, heads * VALUE_DIM), bf16),
             pltpu.VMEM((2, rows, chans), bf16),
+            pltpu.VMEM((rows, width), bf16),
             dma((len(matrices),)),
             dma((2,)),
             dma((2,)),
@@ -624,6 +654,7 @@
             dma((seats,)),
             dma((seats,)),
             dma((seats,)),
+            dma((width // 256,)),
         ],
         compiler_params=pltpu.CompilerParams(
             vmem_limit_bytes=60 << 20, collective_id=0, has_side_effects=True

time: 50.9 us -> 48.6 us (0.955)
  the two profiles are of different devices: /device:TPU:29 before, /device:TPU:25 now
where the time goes in v3:
time: 48.6 us; the launch traced here: 48.3 us
  Pallas kernels  46.2 us (95%)
  local copies, waits for them, and re-layouts  2.06 us (4%)
    pallas_call x1, Pallas kernels, fused(): pl.pallas_call(layer_kernel, out_shape=jax.ShapeDtypeStruct((rows, width)...  46.2 us
    unnamed x1, local copies, waits for them, and re-layouts  2.06 us

profile of v3, /device:TPU:25, one launch (start us, length us, event | category | flops | bytes accessed | tf_op | source)
XLA Modules:
  0.0 48.3 jit_solution(8344027814094485492)
XLA Ops:
  0.0 46.2 %layer.1 = bf16[384,1024]{1,0:T(8,128)(2,1)} custom-call(bf16[384,1024]{1,0:T(8,128)(2,1)} %tok_hbm.1, f32[1,2048]{1,0:T(1,128)} %bitcast.8, f32[1,256]{1,0:T(1,128)} %bitcast.13, f32[32,384]{1,0:T(8,128)} %constant.4.clone.base_ref, f32[32,128]{1,0:T(8,128)} %constant.5.clone.seat_ref, f32[31,512]{1,0:T(8,128)} %taps_ref.1, f32[1,512]{1,0:T(1,128)} %bitcast.9, ...), custom_call_target="tpu_custom_call" | custom-call | tf_op jit(solution)/shard_map/layer/pallas_call | solution.py:609
  46.2 2.1 %copy.22 = bf16[384,1024]{1,0:T(8,128)(2,1)} copy(bf16[384,1024]{1,0:T(8,128)(2,1)} %layer.1) | data formatting | bytes 1572864

commit v4 on v3

--- a/solution.py
+++ b/solution.py
@@ -80,7 +80,8 @@
     att_sq, att_sq_other, att_act, conv_act, out_stage,
     w_sem, w_send, w_recv, tok_load, tok_send, tok_recv, rim_send, rim_recv, sq_send, sq_recv,
     csq_send, csq_recv, asq_send, asq_recv, conv_send, conv_recv, att_send, att_recv,
-    col_send, plane_send, core_send, link_recv, core_recv, out_sem,
+    col_send, down_send, plane_send, core_send, link_recv, core_recv, out_sem,
+    q_help, help_out, help_in, qh_send, qh_recv, help_send, help_recv,
 ):
     mine = lax.axis_index("tp")
     me = lax.axis_index("sp")
@@ -126,23 +127,27 @@
     def at(layer_id, spot_id):
         return {"sp": layer_id * PLANE + spot_id, "tp": mine}
 
+    q_help[...] = jnp.zeros(q_help.shape, jnp.bfloat16)
     barrier = pltpu.get_barrier_semaphore()
     peers = [at(layer, spot_at(d)) for d in range(1, PLANE)] + [other]
     for peer in peers:
         pl.semaphore_signal(barrier, inc=1, device_id=peer, device_id_type=MESH)
     above = at(jnp.minimum(layer + 1, layers - 1), spot)
     below = at(jnp.maximum(layer - 1, 0), spot)
+    top_layer = layers - 1
+    opposite = at(top_layer - layer, spot)
+    outer = jnp.where((layer == 0) | (layer == top_layer), 1, 0)
     for condition, peer in (
-        (layer < layers - 1, above), (layer > 0, below), (me < seats - 1, ahead), (me > 0, behind),
+        (outer == 1, opposite), (layer < layers - 1, above), (layer > 0, below), (me < seats - 1, ahead), (me > 0, behind),
     ):
 
         @pl.when(condition)
         def _(peer=peer):
             pl.semaphore_signal(barrier, inc=1, device_id=peer, device_id_type=MESH)
 
-    q2[...] = jnp.zeros(q2.shape, jnp.bfloat16)
     pairs, _, both = q2.shape
     keys_wide = kn.shape[1]
+    q2[...] = jnp.zeros(q2.shape, jnp.bfloat16)
     ones_low = VALUE_DIM
     ones_high = vt.shape[2] - VALUE_DIM
     vt[:, :, ones_low:ones_high, :] = jnp.ones(
@@ -154,7 +159,8 @@
         + jnp.minimum(me, 1)
         + jnp.minimum(seats - 1 - me, 1)
         + jnp.minimum(layer, 1)
-        + jnp.minimum(layers - 1 - layer, 1),
+        + jnp.minimum(layers - 1 - layer, 1)
+        + outer,
     )
     fetch.wait()
     tok_copy = push(tok, landed, tok_send, tok_recv, other)
@@ -221,6 +227,10 @@
         spread = lat_ref.at[block, half]
         return push(spread, spread, col_send.at[block // PLANE], link_recv.at[block], above)
 
+    def down_copy(block):
+        spread = lat_ref.at[block, half]
+        return push(spread, spread, down_send.at[block // PLANE], link_recv.at[block], below)
+
     def rise(block):
         @pl.when(layer + 1 < layers)
         def _():
@@ -240,6 +250,11 @@
         return push(spread, spread, core_send.at[block], core_recv.at[block], other)
 
     rise(me)
+
+    @pl.when(layer > 0)
+    def _():
+        down_copy(me).start()
+
     for d in range(1, PLANE):
         plane_copy(me, d).start()
     for gift in gifts:
@@ -249,23 +264,41 @@
         spread = lat_ref.at[block, half]
         push(spread, spread, core_send.at[block], link_recv.at[block], other).wait_recv()
 
+    def spread_layer(which, upward):
+        block = which * PLANE + spot
+        arrive(block)
+        if upward:
+            rise(block)
+        for d in range(1, PLANE):
+            plane_copy(block, d).start()
+        core_copy(block).start()
+
+    def hand_layer(which):
+        for d in range(1, PLANE):
+            block = which * PLANE + spot_at(d)
+            arrive(block)
+            core_copy(block).start()
+
     def relay(step):
         @pl.when(step <= layer)
         def _():
-            block = (layer - step) * PLANE + spot
-            arrive(block)
-            rise(block)
-            for d in range(1, PLANE):
-                plane_copy(block, d).start()
-            core_copy(block).start()
+            spread_layer(layer - step, True)
 
     def hand_over(step):
         @pl.when(step <= layer)
         def _():
-            for d in range(1, PLANE):
-                block = (layer - step) * PLANE + spot_at(d)
-                arrive(block)
-                core_copy(block).start()
+            hand_layer(layer - step)
+
+    def descend(distance):
+        @pl.when((layer > 0) & (layer + distance < layers))
+        def _():
+            block = (layer + distance) * PLANE + spot
+            arrive(block)
+            down_copy(block).start()
+
+        @pl.when((layer == 0) & (distance < layers))
+        def _():
+            spread_layer(distance, False)
 
     loads[2].wait()
     loads[3].wait()
@@ -293,6 +326,31 @@
             turned[head * ROT_DIM : (head + 1) * ROT_DIM]
         ).astype(jnp.bfloat16)
 
+    lent = pairs - 1
+    q_parts = tuple(
+        (pl.ds(low, count), pl.ds(first_col, cols))
+        for low, count, first_col, cols in (
+            (0, NOPE_DIM, 0, rows),
+            (NOPE_DIM, NOPE_DIM, rows, rows),
+            (2 * NOPE_DIM, ROT_DIM, 0, 2 * rows),
+        )
+    )
+    q_copies = [
+        push(
+            q2.at[lent, part_rows, part_cols],
+            q_help.at[part_rows, part_cols],
+            qh_send.at[index],
+            qh_recv.at[index],
+            opposite,
+        )
+        for index, (part_rows, part_cols) in enumerate(q_parts)
+    ]
+
+    @pl.when(layer == top_layer)
+    def _():
+        for copy in q_copies:
+            copy.start()
+
     loads[7].wait()
     vup_t[...] = vup[...].astype(jnp.float32).T.astype(jnp.bfloat16)
 
@@ -317,6 +375,7 @@
         lax.fori_loop(1, rows // chunk, functools.partial(band_step, slab=slab), 0)
         if slab == slabs // 2:
             relay(1)
+            descend(1)
     hand_over(0)
 
     @pl.when(me > 0)
@@ -364,7 +423,7 @@
     strip = 256
     strips = keys_wide // strip
 
-    def expand(group, slot, index):
+    def expand(group, slot, index, only=None):
         pieces = []
         low, left = index * strip, strip
         while left > 0:
@@ -375,13 +434,19 @@
             low, left = low + take, left - take
         lat = pieces[0] if len(pieces) == 1 else jnp.concatenate(pieces, axis=0)
         cut = slice(index * strip, (index + 1) * strip)
-        kn[slot, cut, :] = jnp.dot(
-            lat, kup[...], preferred_element_type=jnp.float32
+        some = range(pairs) if only is None else range(only, only + 1)
+        key_cols = slice(2 * NOPE_DIM * some[0], 2 * NOPE_DIM * (some[-1] + 1))
+        value_cols = slice(2 * VALUE_DIM * some[0], 2 * VALUE_DIM * (some[-1] + 1))
+        kn[slot, cut, : 2 * NOPE_DIM * len(some)] = jnp.dot(
+            lat, kup[:, key_cols], preferred_element_type=jnp.float32
         ).astype(jnp.bfloat16)
         values = lax.dot_general(
-            vup_t[...], lat, (((1,), (1,)), ((), ())), preferred_element_type=jnp.float32
+            vup_t[value_cols, :],
+            lat,
+            (((1,), (1,)), ((), ())),
+            preferred_element_type=jnp.float32,
         ).astype(jnp.bfloat16)
-        for pair in range(pairs):
+        for pair in range(len(some)):
             low = 2 * VALUE_DIM * pair
             vt[slot, pair, :ones_low, cut] = values[low : low + VALUE_DIM]
             vt[slot, pair, ones_high:, cut] = values[low + VALUE_DIM : low + 2 * VALUE_DIM]
@@ -404,6 +469,21 @@
         for tile in range(tiles)
     )
 
+    def hidden_keys(first_key, first_query):
+        key = first_key + lax.broadcasted_iota(jnp.int32, (strip, both), 0)
+        query = lax.broadcasted_iota(jnp.int32, (strip, both), 1)
+        return key > first_query + jnp.where(query >= rows, query - rows, query)
+
+    def weigh(slot, place_id, index, weights, sums):
+        cut = slice(index * strip, (index + 1) * strip)
+        for tile, (low, high) in enumerate(tile_rows):
+            new = jnp.dot(
+                vt[slot, place_id, low:high, cut],
+                weights[:, 256 * tile : 256 * (tile + 1)],
+                preferred_element_type=jnp.float32,
+            )
+            sums[tile] = new if sums[tile] is None else sums[tile] + new
+
     def attend(slot, first, hidden, middle, following):
         def score(pair, index):
             cut = slice(index * strip, (index + 1) * strip)
@@ -416,33 +496,21 @@
             s_ref[pair % 2, cut, :] = scores
             return jnp.max(scores, axis=0, keepdims=True)
 
-        tops = [score(0, index) for index in range(strips)]
-        for pair in range(pairs):
-            middle(pair)
-            top = tops[0]
-            for value in tops[1:]:
-                top = jnp.maximum(top, value)
+        def settle_top(pair, tops):
+            top = functools.reduce(jnp.maximum, tops)
+            fade = None
             if not first:
                 old = run_max[pair : pair + 1, :]
                 top = jnp.maximum(old, top)
                 fade = jnp.exp2(old - top)
             run_max[pair : pair + 1, :] = top
-            tops = []
-            sums = [None] * tiles
-            for index in range(strips):
-                cut = slice(index * strip, (index + 1) * strip)
-                if pair + 1 < pairs:
-                    tops.append(score(pair + 1, index))
-                weights = jnp.exp2(s_ref[pair % 2, cut, :] - top).astype(jnp.bfloat16)
-                for tile, (low, high) in enumerate(tile_rows):
-                    new = jnp.dot(
-                        vt[slot, pair, low:high, cut],
-                        weights[:, 256 * tile : 256 * (tile + 1)],
-                        preferred_element_type=jnp.float32,
-                    )
-                    sums[tile] = new if sums[tile] is None else sums[tile] + new
-                if pair + 1 == pairs:
-                    expand(following, 1 - slot, index)
+            return top, fade
+
+        def weights_of(pair, index, top):
+            cut = slice(index * strip, (index + 1) * strip)
+            return jnp.exp2(s_ref[pair % 2, cut, :] - top).astype(jnp.bfloat16)
+
+        def close(pair, sums, fade):
             for tile, (low, high) in enumerate(tile_rows):
                 new = sums[tile]
                 if not first:
@@ -451,48 +519,84 @@
                     ]
                 acc[pair, tile, : high - low, :] = new
 
+        tops = [score(0, index) for index in range(strips)]
+        for pair in range(lent):
+            middle(pair)
+            top, fade = settle_top(pair, tops)
+            tops = []
+            sums = [None] * tiles
+            for index in range(strips):
+                if pair + 1 < lent:
+                    tops.append(score(pair + 1, index))
+                weigh(slot, pair, index, weights_of(pair, index, top), sums)
+                if pair + 1 == lent and following is not None:
+                    expand(following, 1 - slot, index)
+            close(pair, sums, fade)
+
+        @pl.when(layer < top_layer)
+        def _():
+            top, fade = settle_top(lent, [score(lent, index) for index in range(strips)])
+            sums = [None] * tiles
+            for index in range(strips):
+                weigh(slot, lent, index, weights_of(lent, index, top), sums)
+            close(lent, sums, fade)
+
     def hidden(index):
-        key = layer * keys_wide + index * strip + lax.broadcasted_iota(
-            jnp.int32, (strip, both), 0
-        )
-        query = lax.broadcasted_iota(jnp.int32, (strip, both), 1)
-        return key > me * rows + jnp.where(query >= rows, query - rows, query)
+        return hidden_keys(layer * keys_wide + index * strip, me * rows)
 
     loads[6].wait()
     gathered(0)
     for index in range(strips):
         expand(layer, 0, index)
+    for distance in range(2, layers):
+
+        @pl.when(layer > 0)
+        def _(distance=distance):
+            descend(distance)
+
+
+    def ready_layer(which):
+        for d in range(PLANE):
+            core_copy(which * PLANE + spot_at(d)).wait_recv()
 
     def ready(step):
         @pl.when(step <= layer)
         def _():
-            for d in range(PLANE):
-                core_copy((layer - step) * PLANE + spot_at(d)).wait_recv()
+            ready_layer(layer - step)
 
     def first_middle(pair):
-        if pair == pairs // 2:
+        if pair == 1:
             relay(2)
             hand_over(1)
+
+            @pl.when(layer == 0)
+            def _():
+                descend(2)
+
             activate()
-        if pair == pairs - 1:
+        if pair == lent - 1:
             ready(1)
 
     attend(0, True, hidden, first_middle, jnp.maximum(layer - 1, 0))
 
     def far(step, carry):
         def middle(pair):
-            if pair == pairs // 2:
+            if pair == 1:
                 relay(step + 2)
                 hand_over(step + 1)
-            if pair == pairs - 1:
+            if pair == lent - 1:
                 ready(step + 1)
 
-        attend(step % 2, False, None, middle, jnp.maximum(layer - step - 1, 0))
+        attend(step % 2, False, None, middle, layer - step - 1)
         return carry
 
-    lax.fori_loop(1, layer + 1, far, 0)
-
-    for pair in range(pairs):
+    lax.fori_loop(1, layer, far, 0)
+
+    @pl.when(layer > 0)
+    def _():
+        attend(layer % 2, False, None, lambda pair: None, None)
+
+    def finish(pair, keep):
         for side in range(2):
             pieces = []
             for tile, (low, high) in enumerate(tile_rows):
@@ -505,10 +609,84 @@
                 pieces.append(
                     total[base : base + VALUE_DIM] / total[ones_low - low : ones_low - low + 1]
                 )
+            keep(side, jnp.concatenate(pieces, axis=1).astype(jnp.bfloat16))
+
+    def keep_local(pair):
+        def keep(side, block):
             low = (2 * pair + side) * VALUE_DIM
-            att_t[low : low + VALUE_DIM, :] = (
-                jnp.concatenate(pieces, axis=1).astype(jnp.bfloat16).astype(jnp.float32)
-            )
+            att_t[low : low + VALUE_DIM, :] = block.astype(jnp.float32)
+
+        return keep
+
+    for pair in range(lent):
+        finish(pair, keep_local(pair))
+
+    @pl.when(layer < top_layer)
+    def _():
+        finish(lent, keep_local(lent))
+
+    help_copy = push(help_out, help_in, help_send, help_recv, opposite)
+
+    @pl.when(layer == 0)
+    def _():
+        for distance in range(3, layers):
+            descend(distance)
+        for copy in q_copies:
+            copy.wait_recv()
+        run_max[0:1, :] = jnp.full((1, both), far_below, jnp.float32)
+        acc[0] = jnp.zeros(acc.shape[1:], jnp.float32)
+        guest = top_layer * PLANE + spot
+
+        def lend(which, carry):
+            @pl.when(which + 1 < layers)
+            def _():
+                hand_layer(which + 1)
+
+            @pl.when(which > 0)
+            def _():
+                ready_layer(which)
+
+            tops = []
+            for index in range(strips):
+                expand(which, 0, index, lent)
+            for index in range(strips):
+                cut = slice(index * strip, (index + 1) * strip)
+                keys = jnp.concatenate([kn[0, cut, :128], kr[0, cut, :]], axis=1)
+                scores = jnp.dot(keys, q_help[...], preferred_element_type=jnp.float32)
+                scores = jnp.where(
+                    hidden_keys(which * keys_wide + index * strip, guest * rows), far_below, scores
+                )
+                s_ref[0, cut, :] = scores
+                tops.append(jnp.max(scores, axis=0, keepdims=True))
+            old = run_max[0:1, :]
+            top = jnp.maximum(old, functools.reduce(jnp.maximum, tops))
+            fade = jnp.exp2(old - top)
+            run_max[0:1, :] = top
+            sums = [None] * tiles
+            for index in range(strips):
+                cut = slice(index * strip, (index + 1) * strip)
+                weights = jnp.exp2(s_ref[0, cut, :] - top).astype(jnp.bfloat16)
+                weigh(0, 0, index, weights, sums)
+            for tile, (low, high) in enumerate(tile_rows):
+                acc[0, tile, : high - low, :] = sums[tile] + acc[0, tile, : high - low, :] * fade[
+                    :, 256 * tile : 256 * (tile + 1)
+                ]
+            return carry
+
+        lax.fori_loop(0, layers, lend, 0)
+
+        def keep(side, block):
+            help_out[side * VALUE_DIM : (side + 1) * VALUE_DIM, :] = block
+
+        finish(0, keep)
+        help_copy.start()
+
+    @pl.when(layer == top_layer)
+    def _():
+        help_copy.wait_recv()
+        low = 2 * lent * VALUE_DIM
+        att_t[low : low + 2 * VALUE_DIM, :] = help_in[...].astype(jnp.float32)
+
     attended = att_t[...]
     att_sq[...] = jnp.broadcast_to(
         jnp.sum(attended * attended, axis=0, keepdims=True), att_sq.shape
@@ -571,6 +749,32 @@
         return carry
 
     lax.fori_loop(0, layer + 1, settle, 0)
+
+    def settle_down(which, carry):
+        down_copy(which * PLANE + spot).wait_send()
+        return carry
+
+    @pl.when(layer > 0)
+    def _():
+        lax.fori_loop(layer, layers, settle_down, 0)
+
+    def settle_guest(which, carry):
+        for d in range(1, PLANE):
+            plane_copy(which * PLANE + spot, d).wait_send()
+        for d in range(PLANE):
+            core_copy(which * PLANE + spot_at(d)).wait_send()
+        return carry
+
+    @pl.when(layer == 0)
+    def _():
+        lax.fori_loop(1, layers, settle_guest, 0)
+        help_copy.wait_send()
+
+    @pl.when(layer == top_layer)
+    def _():
+        for copy in q_copies:
+            copy.wait_send()
+
     for leave in leaves:
         leave.wait()
 
@@ -650,11 +854,19 @@
         + [dma] * 15
         + [
             dma((layers,)),
+            dma((layers,)),
             dma((layers, PLANE - 1)),
             dma((seats,)),
             dma((seats,)),
             dma((seats,)),
             dma((width // 256,)),
+            pltpu.VMEM((256, 2 * rows), bf16),
+            pltpu.VMEM((2 * VALUE_DIM, rows), bf16),
+            pltpu.VMEM((2 * VALUE_DIM, rows), bf16),
+            dma((3,)),
+            dma((3,)),
+            dma,
+            dma,
         ],
         compiler_params=pltpu.CompilerParams(
             vmem_limit_bytes=60 << 20, collective_id=0, has_side_effects=True
@@ -832,6 +1044,8 @@
         and seats % PLANE == 0
         and tok_rows % 128 == 0
         and heads_here % 2 == 0
+        and heads_here > 2
+        and seats > PLANE
     ):
         gains = (
             input_gain, kv_gain, conv_ln_gain, conv_ln_bias, att_out_gain, conv_out_gain

time: 48.6 us -> 47.3 us (0.973)
  Pallas kernels: 46.2 us -> 45 us
    pallas_call x1, Pallas kernels: 46.2 us -> 45 us  [fused(): pl.pallas_call(layer_kernel, out_shape=jax.ShapeDtypeStruct((rows, width)...]
where the time goes in v4:
time: 47.3 us; the launch traced here: 47.1 us
  Pallas kernels  45 us (95%)
  local copies, waits for them, and re-layouts  2.06 us (4%)
    pallas_call x1, Pallas kernels, fused(): pl.pallas_call(layer_kernel, out_shape=jax.ShapeDtypeStruct((rows, width)...  45 us
    unnamed x1, local copies, waits for them, and re-layouts  2.06 us

profile of v4, /device:TPU:25, one launch (start us, length us, event | category | flops | bytes accessed | tf_op | source)
XLA Modules:
  0.0 47.1 jit_solution(4786091689593589373)
XLA Ops:
  0.0 45.0 %layer.1 = bf16[384,1024]{1,0:T(8,128)(2,1)} custom-call(bf16[384,1024]{1,0:T(8,128)(2,1)} %tok_hbm.1, f32[1,2048]{1,0:T(1,128)} %bitcast.8, f32[1,256]{1,0:T(1,128)} %bitcast.13, f32[32,384]{1,0:T(8,128)} %constant.4.clone.base_ref, f32[32,128]{1,0:T(8,128)} %constant.5.clone.seat_ref, f32[31,512]{1,0:T(8,128)} %taps_ref.1, f32[1,512]{1,0:T(1,128)} %bitcast.9, ...), custom_call_target="tpu_custom_call" | custom-call | tf_op jit(solution)/shard_map/layer/pallas_call | solution.py:813
  45.0 2.1 %copy.22 = bf16[384,1024]{1,0:T(8,128)(2,1)} copy(bf16[384,1024]{1,0:T(8,128)(2,1)} %layer.1) | data formatting | bytes 1572864

commit v5 on v4

--- a/solution.py
+++ b/solution.py
@@ -69,15 +69,18 @@
 PLANE = 4
 
 
+FAR_FIRST = (3, 1, 2)
+
+
 def layer_kernel(
     tok_hbm, gain_ref, kv_gain_ref, base_ref, seat_ref, taps_ref, ln_gain_ref, ln_bias_ref,
     att_gain_ref, conv_gain_ref,
     kvd_hbm, rotw_hbm, cgw_hbm, cvw_hbm, qw_hbm, qrw_hbm, kup_hbm, vup_hbm, att_hbm, conv_hbm,
     out_ref,
     kvd, rotw, cgw, cvw, qw, qrw, kup, vup, att_w, conv_w, vup_t,
-    tok, landed, scaled, narrow, gated, rim, wide, conv, sq_mine, sq_other,
+    tok, landed, scaled, own_raw, narrow, gated, rim, wide, conv, sq_mine, sq_other,
     lat_ref, q2, kn, kr, vt, run_max, acc, s_ref, att_t, end_mine, end_other,
-    att_sq, att_sq_other, att_act, conv_act, out_stage,
+    att_sq, att_sq_other, att_act, conv_act, out_stage, base_part, own_part,
     w_sem, w_send, w_recv, tok_load, tok_send, tok_recv, rim_send, rim_recv, sq_send, sq_recv,
     csq_send, csq_recv, asq_send, asq_recv, conv_send, conv_recv, att_send, att_recv,
     col_send, down_send, plane_send, core_send, link_recv, core_recv, out_sem,
@@ -121,8 +124,8 @@
         for index, (src, dst) in enumerate(((att_hbm, att_w), (conv_hbm, conv_w)))
     ]
 
-    def spot_at(distance):
-        return (spot + distance) % PLANE
+    def spot_at(step):
+        return (spot % 2 + step % 2) % 2 + 2 * ((spot // 2 + step // 2) % 2)
 
     def at(layer_id, spot_id):
         return {"sp": layer_id * PLANE + spot_id, "tp": mine}
@@ -136,10 +139,12 @@
     below = at(jnp.maximum(layer - 1, 0), spot)
     top_layer = layers - 1
     opposite = at(top_layer - layer, spot)
-    outer = jnp.where((layer == 0) | (layer == top_layer), 1, 0)
-    for condition, peer in (
-        (outer == 1, opposite), (layer < layers - 1, above), (layer > 0, below), (me < seats - 1, ahead), (me > 0, behind),
-    ):
+    root = at(0, spot)
+    for condition, peer in [
+        (layer == 0, at(other_layer, spot)) for other_layer in range(2, layers)
+    ] + [
+        (layer > 1, root), (layer < layers - 1, above), (layer > 0, below), (me < seats - 1, ahead), (me > 0, behind),
+    ]:
 
         @pl.when(condition)
         def _(peer=peer):
@@ -160,7 +165,7 @@
         + jnp.minimum(seats - 1 - me, 1)
         + jnp.minimum(layer, 1)
         + jnp.minimum(layers - 1 - layer, 1)
-        + outer,
+        + jnp.where(layer == 0, layers - 2, jnp.where(layer > 1, 1, 0)),
     )
     fetch.wait()
     tok_copy = push(tok, landed, tok_send, tok_recv, other)
@@ -192,6 +197,10 @@
             [front * cos_table - back * sin_table, back * cos_table + front * sin_table], axis=0
         )
 
+    loads[0].wait()
+    own_raw[...] = jnp.dot(
+        scaled[:, columns(mine)], kvd[columns(mine), :], preferred_element_type=jnp.float32
+    )
     tok_copy.wait()
     squares = squares + place(landed, 1 - mine)
     row_scale = lax.rsqrt(squares / (2 * width) + norm_eps)
@@ -199,9 +208,10 @@
     def project(weight):
         return jnp.dot(scaled[...], weight[...], preferred_element_type=jnp.float32)
 
-    loads[0].wait()
     loads[1].wait()
-    raw = project(kvd)
+    raw = own_raw[...] + jnp.dot(
+        scaled[:, columns(1 - mine)], kvd[columns(1 - mine), :], preferred_element_type=jnp.float32
+    )
     latent = (
         raw
         * lax.rsqrt(jnp.mean(raw * raw, axis=1, keepdims=True) + norm_eps)
@@ -227,9 +237,9 @@
         spread = lat_ref.at[block, half]
         return push(spread, spread, col_send.at[block // PLANE], link_recv.at[block], above)
 
-    def down_copy(block):
-        spread = lat_ref.at[block, half]
-        return push(spread, spread, down_send.at[block // PLANE], link_recv.at[block], below)
+    down_copy = push(
+        lat_ref.at[me, half], lat_ref.at[me, half], down_send, link_recv.at[me], root
+    )
 
     def rise(block):
         @pl.when(layer + 1 < layers)
@@ -253,9 +263,9 @@
 
     @pl.when(layer > 0)
     def _():
-        down_copy(me).start()
-
-    for d in range(1, PLANE):
+        down_copy.start()
+
+    for d in FAR_FIRST:
         plane_copy(me, d).start()
     for gift in gifts:
         gift.start()
@@ -269,7 +279,7 @@
         arrive(block)
         if upward:
             rise(block)
-        for d in range(1, PLANE):
+        for d in FAR_FIRST:
             plane_copy(block, d).start()
         core_copy(block).start()
 
@@ -290,12 +300,6 @@
             hand_layer(layer - step)
 
     def descend(distance):
-        @pl.when((layer > 0) & (layer + distance < layers))
-        def _():
-            block = (layer + distance) * PLANE + spot
-            arrive(block)
-            down_copy(block).start()
-
         @pl.when((layer == 0) & (distance < layers))
         def _():
             spread_layer(distance, False)
@@ -548,11 +552,8 @@
     gathered(0)
     for index in range(strips):
         expand(layer, 0, index)
-    for distance in range(2, layers):
-
-        @pl.when(layer > 0)
-        def _(distance=distance):
-            descend(distance)
+    descend(2)
+    relay(2)
 
 
     def ready_layer(which):
@@ -566,13 +567,10 @@
 
     def first_middle(pair):
         if pair == 1:
-            relay(2)
             hand_over(1)
 
-            @pl.when(layer == 0)
-            def _():
-                descend(2)
-
+            for distance in range(3, layers):
+                descend(distance)
             activate()
         if pair == lent - 1:
             ready(1)
@@ -581,8 +579,9 @@
 
     def far(step, carry):
         def middle(pair):
+            if pair == 0:
+                relay(step + 2)
             if pair == 1:
-                relay(step + 2)
                 hand_over(step + 1)
             if pair == lent - 1:
                 ready(step + 1)
@@ -629,8 +628,6 @@
 
     @pl.when(layer == 0)
     def _():
-        for distance in range(3, layers):
-            descend(distance)
         for copy in q_copies:
             copy.wait_recv()
         run_max[0:1, :] = jnp.full((1, both), far_below, jnp.float32)
@@ -681,21 +678,6 @@
         finish(0, keep)
         help_copy.start()
 
-    @pl.when(layer == top_layer)
-    def _():
-        help_copy.wait_recv()
-        low = 2 * lent * VALUE_DIM
-        att_t[low : low + 2 * VALUE_DIM, :] = help_in[...].astype(jnp.float32)
-
-    attended = att_t[...]
-    att_sq[...] = jnp.broadcast_to(
-        jnp.sum(attended * attended, axis=0, keepdims=True), att_sq.shape
-    )
-    att_act[0] = (attended.T * att_gain_ref[...]).astype(jnp.bfloat16)
-    att_sum = push(att_sq, att_sq_other, asq_send, asq_recv, other)
-    att_sum.start()
-    att_copy = push(att_act.at[0], att_act.at[1], att_send, att_recv, other)
-    att_copy.start()
     for index in (8, 9):
         loads[index].wait()
     for gift in gifts:
@@ -707,27 +689,32 @@
     def product(activations, weight):
         return jnp.dot(activations, weight, preferred_element_type=jnp.float32)
 
-    base_part = (
+    bulk = 2 * lent * VALUE_DIM
+    total_width = bulk + 2 * VALUE_DIM
+
+    def hand_in(low, high, slot):
+        attended = att_t[low:high, :]
+        att_act[0, :, low:high] = (attended.T * att_gain_ref[:, low:high]).astype(jnp.bfloat16)
+        copy = push(
+            att_act.at[0, :, pl.ds(low, high - low)],
+            att_act.at[1, :, pl.ds(low, high - low)],
+            att_send.at[slot],
+            att_recv.at[slot],
+            other,
+        )
+        copy.start()
+        return copy, jnp.sum(attended * attended, axis=0, keepdims=True)
+
+    def share(core, low, high):
+        return product(att_act[core, :, low:high], att_w[core, low:high, :])
+
+    bulk_copy, bulk_sq = hand_in(0, bulk, 0)
+    att_sq[...] = jnp.broadcast_to(bulk_sq, att_sq.shape)
+    base_part[...] = (
         product(conv_act[0], conv_w[0]) + product(conv_act[1], conv_w[1])
     ) * conv_scale
-    own_part = product(att_act[0], att_w[0])
-    att_sum.wait()
-    squares_t = jnp.broadcast_to(att_sq[:1] + att_sq_other[:1], (128, rows)).T
-    att_scale = lax.rsqrt(squares_t[:, :1] / ATT_WIDTH + norm_eps)
-    att_copy.wait()
-    leaves = []
-    for index in range(width // 256):
-        cols = slice(index * 256, (index + 1) * 256)
-        out_stage[:, cols] = (
-            (own_part[:, cols] + product(att_act[1], att_w[1, :, cols])) * att_scale
-            + base_part[:, cols]
-        ).astype(jnp.bfloat16)
-        leave = pltpu.make_async_copy(
-            out_stage.at[:, cols], out_ref.at[:, cols], out_sem.at[index]
-        )
-        leave.start()
-        leaves.append(leave)
-
+    own_part[...] = share(0, 0, bulk)
+    bulk_copy.wait()
     @pl.when(me < seats - 1)
     def _():
         rim_copy.wait_send()
@@ -750,13 +737,9 @@
 
     lax.fori_loop(0, layer + 1, settle, 0)
 
-    def settle_down(which, carry):
-        down_copy(which * PLANE + spot).wait_send()
-        return carry
-
     @pl.when(layer > 0)
     def _():
-        lax.fori_loop(layer, layers, settle_down, 0)
+        down_copy.wait_send()
 
     def settle_guest(which, carry):
         for d in range(1, PLANE):
@@ -774,6 +757,37 @@
     def _():
         for copy in q_copies:
             copy.wait_send()
+
+    @pl.when(layer == top_layer)
+    def _():
+        help_copy.wait_recv()
+        att_t[bulk:total_width, :] = help_in[...].astype(jnp.float32)
+
+    rest_copy, rest_sq = hand_in(bulk, total_width, 1)
+    att_sq[...] = att_sq[...] + rest_sq
+    att_sum = push(att_sq, att_sq_other, asq_send, asq_recv, other)
+    att_sum.start()
+    own_part[...] = own_part[...] + share(1, 0, bulk) + share(0, bulk, total_width)
+    att_sum.wait()
+    squares_t = jnp.broadcast_to(att_sq[:1] + att_sq_other[:1], (128, rows)).T
+    att_scale = lax.rsqrt(squares_t[:, :1] / ATT_WIDTH + norm_eps)
+    rest_copy.wait()
+    leaves = []
+    for index in range(width // 256):
+        cols = slice(index * 256, (index + 1) * 256)
+        out_stage[:, cols] = (
+            (
+                own_part[:, cols]
+                + product(att_act[1, :, bulk:total_width], att_w[1, bulk:total_width, cols])
+            )
+            * att_scale
+            + base_part[:, cols]
+        ).astype(jnp.bfloat16)
+        leave = pltpu.make_async_copy(
+            out_stage.at[:, cols], out_ref.at[:, cols], out_sem.at[index]
+        )
+        leave.start()
+        leaves.append(leave)
 
     for leave in leaves:
         leave.wait()
@@ -824,6 +838,7 @@
             pltpu.VMEM((rows, width), bf16),
             pltpu.VMEM((rows, width), bf16),
             pltpu.VMEM((rows, 2 * width), bf16),
+            pltpu.VMEM((rows, rank), f32),
             pltpu.VMEM((rows, 128), f32),
             pltpu.VMEM((rows, chans), bf16),
             pltpu.VMEM((edge, chans), bf16),
@@ -847,14 +862,18 @@
             pltpu.VMEM((2, rows, heads * VALUE_DIM), bf16),
             pltpu.VMEM((2, rows, chans), bf16),
             pltpu.VMEM((rows, width), bf16),
+            pltpu.VMEM((rows, width), f32),
+            pltpu.VMEM((rows, width), f32),
             dma((len(matrices),)),
             dma((2,)),
             dma((2,)),
         ]
-        + [dma] * 15
+        + [dma] * 13
         + [
+            dma((2,)),
+            dma((2,)),
             dma((layers,)),
-            dma((layers,)),
+            dma,
             dma((layers, PLANE - 1)),
             dma((seats,)),
             dma((seats,)),

time: 47.3 us -> 49.4 us (1.044)
  Pallas kernels: 45 us -> 46.8 us
    pallas_call x1, Pallas kernels: 45 us -> 46.8 us  [fused(): pl.pallas_call(layer_kernel, out_shape=jax.ShapeDtypeStruct((rows, width)...]
where the time goes in v5:
time: 49.4 us; the launch traced here: 48.9 us
  Pallas kernels  46.8 us (95%)
  local copies, waits for them, and re-layouts  2.06 us (4%)
    pallas_call x1, Pallas kernels, fused(): pl.pallas_call(layer_kernel, out_shape=jax.ShapeDtypeStruct((rows, width)...  46.8 us
    unnamed x1, local copies, waits for them, and re-layouts  2.06 us

profile of v5, /device:TPU:25, one launch (start us, length us, event | category | flops | bytes accessed | tf_op | source)
XLA Modules:
  0.0 48.9 jit_solution(8122411319016658512)
XLA Ops:
  0.0 46.8 %layer.1 = bf16[384,1024]{1,0:T(8,128)(2,1)} custom-call(bf16[384,1024]{1,0:T(8,128)(2,1)} %tok_hbm.1, f32[1,2048]{1,0:T(1,128)} %bitcast.8, f32[1,256]{1,0:T(1,128)} %bitcast.13, f32[32,384]{1,0:T(8,128)} %constant.4.clone.base_ref, f32[32,128]{1,0:T(8,128)} %constant.5.clone.seat_ref, f32[31,512]{1,0:T(8,128)} %taps_ref.1, f32[1,512]{1,0:T(1,128)} %bitcast.9, ...), custom_call_target="tpu_custom_call" | custom-call | tf_op jit(solution)/shard_map/layer/pallas_call | solution.py:827
  46.8 2.1 %copy.22 = bf16[384,1024]{1,0:T(8,128)(2,1)} copy(bf16[384,1024]{1,0:T(8,128)(2,1)} %layer.1) | data formatting | bytes 1572864

commit v6 on v5

--- a/solution.py
+++ b/solution.py
@@ -237,9 +237,11 @@
         spread = lat_ref.at[block, half]
         return push(spread, spread, col_send.at[block // PLANE], link_recv.at[block], above)
 
-    down_copy = push(
-        lat_ref.at[me, half], lat_ref.at[me, half], down_send, link_recv.at[me], root
-    )
+    def down_copy(block, target):
+        spread = lat_ref.at[block, half]
+        return push(spread, spread, down_send.at[block // PLANE], link_recv.at[block], target)
+
+    lower = at(jnp.where(layer == top_layer, 0, jnp.maximum(layer - 1, 0)), spot)
 
     def rise(block):
         @pl.when(layer + 1 < layers)
@@ -263,7 +265,7 @@
 
     @pl.when(layer > 0)
     def _():
-        down_copy.start()
+        down_copy(me, lower).start()
 
     for d in FAR_FIRST:
         plane_copy(me, d).start()
@@ -300,6 +302,12 @@
             hand_layer(layer - step)
 
     def descend(distance):
+        @pl.when((layer > 0) & (layer + distance < top_layer))
+        def _():
+            block = (layer + distance) * PLANE + spot
+            arrive(block)
+            down_copy(block, below).start()
+
         @pl.when((layer == 0) & (distance < layers))
         def _():
             spread_layer(distance, False)
@@ -552,7 +560,17 @@
     gathered(0)
     for index in range(strips):
         expand(layer, 0, index)
-    descend(2)
+    for distance in range(2, layers - 2):
+
+        @pl.when(layer > 0)
+        def _(distance=distance):
+            descend(distance)
+
+    @pl.when(layer == 0)
+    def _():
+        if layers > 2:
+            descend(layers - 1)
+
     relay(2)
 
 
@@ -569,8 +587,12 @@
         if pair == 1:
             hand_over(1)
 
-            for distance in range(3, layers):
-                descend(distance)
+
+            @pl.when(layer == 0)
+            def _():
+                for distance in range(2, layers - 1):
+                    descend(distance)
+
             activate()
         if pair == lent - 1:
             ready(1)
@@ -634,12 +656,19 @@
         acc[0] = jnp.zeros(acc.shape[1:], jnp.float32)
         guest = top_layer * PLANE + spot
 
-        def lend(which, carry):
-            @pl.when(which + 1 < layers)
+        def visited(turn_id):
+            return jnp.where(
+                turn_id <= 1, turn_id, jnp.where(turn_id == 2, top_layer, turn_id - 1)
+            )
+
+        def lend(turn_id, carry):
+            which = visited(turn_id)
+
+            @pl.when(turn_id + 1 < layers)
             def _():
-                hand_layer(which + 1)
-
-            @pl.when(which > 0)
+                hand_layer(visited(turn_id + 1))
+
+            @pl.when(turn_id > 0)
             def _():
                 ready_layer(which)
 
@@ -739,7 +768,13 @@
 
     @pl.when(layer > 0)
     def _():
-        down_copy.wait_send()
+        down_copy(me, lower).wait_send()
+
+        def settle_down(which, carry):
+            down_copy(which * PLANE + spot, below).wait_send()
+            return carry
+
+        lax.fori_loop(layer + 1, top_layer, settle_down, 0)
 
     def settle_guest(which, carry):
         for d in range(1, PLANE):
@@ -873,7 +908,7 @@
             dma((2,)),
             dma((2,)),
             dma((layers,)),
-            dma,
+            dma((layers,)),
             dma((layers, PLANE - 1)),
             dma((seats,)),
             dma((seats,)),

time: 49.4 us -> 45.2 us (0.915)
  Pallas kernels: 46.8 us -> 42.9 us
    pallas_call x1, Pallas kernels: 46.8 us -> 42.9 us  [fused(): pl.pallas_call(layer_kernel, out_shape=jax.ShapeDtypeStruct((rows, width)...]
where the time goes in v6:
time: 45.2 us; the launch traced here: 45 us
  Pallas kernels  42.9 us (95%)
  local copies, waits for them, and re-layouts  2.06 us (5%)
    pallas_call x1, Pallas kernels, fused(): pl.pallas_call(layer_kernel, out_shape=jax.ShapeDtypeStruct((rows, width)...  42.9 us
    unnamed x1, local copies, waits for them, and re-layouts  2.06 us

profile of v6, /device:TPU:25, one launch (start us, length us, event | category | flops | bytes accessed | tf_op | source)
XLA Modules:
  0.0 45.0 jit_solution(17293893164363467253)
XLA Ops:
  0.0 42.9 %layer.1 = bf16[384,1024]{1,0:T(8,128)(2,1)} custom-call(bf16[384,1024]{1,0:T(8,128)(2,1)} %tok_hbm.1, f32[1,2048]{1,0:T(1,128)} %bitcast.8, f32[1,256]{1,0:T(1,128)} %bitcast.13, f32[32,384]{1,0:T(8,128)} %constant.4.clone.base_ref, f32[32,128]{1,0:T(8,128)} %constant.5.clone.seat_ref, f32[31,512]{1,0:T(8,128)} %taps_ref.1, f32[1,512]{1,0:T(1,128)} %bitcast.9, ...), custom_call_target="tpu_custom_call" | custom-call | tf_op jit(solution)/shard_map/layer/pallas_call | solution.py:862
  42.9 2.1 %copy.22 = bf16[384,1024]{1,0:T(8,128)(2,1)} copy(bf16[384,1024]{1,0:T(8,128)(2,1)} %layer.1) | data formatting | bytes 1572864

commit v7 on v6

--- a/solution.py
+++ b/solution.py
@@ -743,55 +743,6 @@
         product(conv_act[0], conv_w[0]) + product(conv_act[1], conv_w[1])
     ) * conv_scale
     own_part[...] = share(0, 0, bulk)
-    bulk_copy.wait()
-    @pl.when(me < seats - 1)
-    def _():
-        rim_copy.wait_send()
-
-    def settle(step, carry):
-        base = (layer - step) * PLANE
-        for d in range(1, PLANE):
-            plane_copy(base + spot, d).wait_send()
-            core_copy(base + spot_at(d)).wait_send()
-
-        @pl.when(layer + 1 < layers)
-        def _():
-            column_copy(base + spot).wait_send()
-
-        @pl.when(step > 0)
-        def _():
-            core_copy(base + spot).wait_send()
-
-        return carry
-
-    lax.fori_loop(0, layer + 1, settle, 0)
-
-    @pl.when(layer > 0)
-    def _():
-        down_copy(me, lower).wait_send()
-
-        def settle_down(which, carry):
-            down_copy(which * PLANE + spot, below).wait_send()
-            return carry
-
-        lax.fori_loop(layer + 1, top_layer, settle_down, 0)
-
-    def settle_guest(which, carry):
-        for d in range(1, PLANE):
-            plane_copy(which * PLANE + spot, d).wait_send()
-        for d in range(PLANE):
-            core_copy(which * PLANE + spot_at(d)).wait_send()
-        return carry
-
-    @pl.when(layer == 0)
-    def _():
-        lax.fori_loop(1, layers, settle_guest, 0)
-        help_copy.wait_send()
-
-    @pl.when(layer == top_layer)
-    def _():
-        for copy in q_copies:
-            copy.wait_send()
 
     @pl.when(layer == top_layer)
     def _():
@@ -802,6 +753,7 @@
     att_sq[...] = att_sq[...] + rest_sq
     att_sum = push(att_sq, att_sq_other, asq_send, asq_recv, other)
     att_sum.start()
+    bulk_copy.wait()
     own_part[...] = own_part[...] + share(1, 0, bulk) + share(0, bulk, total_width)
     att_sum.wait()
     squares_t = jnp.broadcast_to(att_sq[:1] + att_sq_other[:1], (128, rows)).T
@@ -823,6 +775,55 @@
         )
         leave.start()
         leaves.append(leave)
+
+    @pl.when(me < seats - 1)
+    def _():
+        rim_copy.wait_send()
+
+    def settle(step, carry):
+        base = (layer - step) * PLANE
+        for d in range(1, PLANE):
+            plane_copy(base + spot, d).wait_send()
+            core_copy(base + spot_at(d)).wait_send()
+
+        @pl.when(layer + 1 < layers)
+        def _():
+            column_copy(base + spot).wait_send()
+
+        @pl.when(step > 0)
+        def _():
+            core_copy(base + spot).wait_send()
+
+        return carry
+
+    lax.fori_loop(0, layer + 1, settle, 0)
+
+    @pl.when(layer > 0)
+    def _():
+        down_copy(me, lower).wait_send()
+
+        def settle_down(which, carry):
+            down_copy(which * PLANE + spot, below).wait_send()
+            return carry
+
+        lax.fori_loop(layer + 1, top_layer, settle_down, 0)
+
+    def settle_guest(which, carry):
+        for d in range(1, PLANE):
+            plane_copy(which * PLANE + spot, d).wait_send()
+        for d in range(PLANE):
+            core_copy(which * PLANE + spot_at(d)).wait_send()
+        return carry
+
+    @pl.when(layer == 0)
+    def _():
+        lax.fori_loop(1, layers, settle_guest, 0)
+        help_copy.wait_send()
+
+    @pl.when(layer == top_layer)
+    def _():
+        for copy in q_copies:
+            copy.wait_send()
 
     for leave in leaves:
         leave.wait()

time: 45.2 us -> 44.9 us (level)
  no operation moved by 1% of the time
where the time goes in v7:
time: 44.9 us; the launch traced here: 44.7 us
  Pallas kernels  42.6 us (95%)
  local copies, waits for them, and re-layouts  2.06 us (5%)
    pallas_call x1, Pallas kernels, fused(): pl.pallas_call(layer_kernel, out_shape=jax.ShapeDtypeStruct((rows, width)...  42.6 us
    unnamed x1, local copies, waits for them, and re-layouts  2.06 us

profile of v7, /device:TPU:25, one launch (start us, length us, event | category | flops | bytes accessed | tf_op | source)
XLA Modules:
  0.0 44.7 jit_solution(15968563306631793464)
XLA Ops:
  0.0 42.6 %layer.1 = bf16[384,1024]{1,0:T(8,128)(2,1)} custom-call(bf16[384,1024]{1,0:T(8,128)(2,1)} %tok_hbm.1, f32[1,2048]{1,0:T(1,128)} %bitcast.8, f32[1,256]{1,0:T(1,128)} %bitcast.13, f32[32,384]{1,0:T(8,128)} %constant.4.clone.base_ref, f32[32,128]{1,0:T(8,128)} %constant.5.clone.seat_ref, f32[31,512]{1,0:T(8,128)} %taps_ref.1, f32[1,512]{1,0:T(1,128)} %bitcast.9, ...), custom_call_target="tpu_custom_call" | custom-call | tf_op jit(solution)/shard_map/layer/pallas_call | solution.py:863
  42.6 2.1 %copy.22 = bf16[384,1024]{1,0:T(8,128)(2,1)} copy(bf16[384,1024]{1,0:T(8,128)(2,1)} %layer.1) | data formatting | bytes 1572864

commit v8 on v7

--- a/solution.py
+++ b/solution.py
@@ -358,11 +358,6 @@
         for index, (part_rows, part_cols) in enumerate(q_parts)
     ]
 
-    @pl.when(layer == top_layer)
-    def _():
-        for copy in q_copies:
-            copy.start()
-
     loads[7].wait()
     vup_t[...] = vup[...].astype(jnp.float32).T.astype(jnp.bfloat16)
 
@@ -389,6 +384,11 @@
             relay(1)
             descend(1)
     hand_over(0)
+
+    @pl.when(layer == top_layer)
+    def _():
+        for copy in q_copies:
+            copy.start()
 
     @pl.when(me > 0)
     def _():

time: 44.9 us -> 44.9 us (level)
  no operation moved by 1% of the time
where the time goes in v8:
time: 44.9 us; the launch traced here: 44.7 us
  Pallas kernels  42.6 us (95%)
  local copies, waits for them, and re-layouts  2.06 us (5%)
    pallas_call x1, Pallas kernels, fused(): pl.pallas_call(layer_kernel, out_shape=jax.ShapeDtypeStruct((rows, width)...  42.6 us
    unnamed x1, local copies, waits for them, and re-layouts  2.06 us

profile of v8, /device:TPU:25, one launch (start us, length us, event | category | flops | bytes accessed | tf_op | source)
XLA Modules:
  0.0 44.7 jit_solution(13494923528904416282)
XLA Ops:
  0.0 42.6 %layer.1 = bf16[384,1024]{1,0:T(8,128)(2,1)} custom-call(bf16[384,1024]{1,0:T(8,128)(2,1)} %tok_hbm.1, f32[1,2048]{1,0:T(1,128)} %bitcast.8, f32[1,256]{1,0:T(1,128)} %bitcast.13, f32[32,384]{1,0:T(8,128)} %constant.4.clone.base_ref, f32[32,128]{1,0:T(8,128)} %constant.5.clone.seat_ref, f32[31,512]{1,0:T(8,128)} %taps_ref.1, f32[1,512]{1,0:T(1,128)} %bitcast.9, ...), custom_call_target="tpu_custom_call" | custom-call | tf_op jit(solution)/shard_map/layer/pallas_call | solution.py:863
  42.6 2.1 %copy.22 = bf16[384,1024]{1,0:T(8,128)(2,1)} copy(bf16[384,1024]{1,0:T(8,128)(2,1)} %layer.1) | data formatting | bytes 1572864
